TPU v7x, 256 devices: a whole 4x4x8 slice. The times are simulated.
256 devices in a mesh: fs: 16 (over y, x), tp: 16 (over z, core).
Axes of the slice: x: 4, y: 4, z: 8, core: 2. Of those that a mesh axis runs over, the one named last changes fastest.
Arguments:
- tokens: bfloat16 [32768, 2048], P(('fs', 'tp')), may hold values from -24 to 24
- up_gate: bfloat16 [32768, 5632], P('fs', 'tp'), may hold values from -8 to 8
- up_val: bfloat16 [32768, 5632], P('fs', 'tp'), may hold values from -6 to 6
- gate_weight: bfloat16 [2048, 5632], P('fs', 'tp'), may hold values from -0.125 to 0.125
- val_weight: bfloat16 [2048, 5632], P('fs', 'tp'), may hold values from -0.125 to 0.125
- gate_taps: bfloat16 [3, 5632], P(None, 'tp'), may hold values from -3 to 3
- val_taps: bfloat16 [3, 5632], P(None, 'tp'), may hold values from -3 to 3
- hidden_grad: bfloat16 [32768, 5632], P('fs', 'tp'), may hold values from -6 to 6
Outputs:
- input_grad: bfloat16 [32768, 2048], P(('fs', 'tp'))
- gate_weight_grad: float32 [2048, 5632], P('fs', 'tp')
- val_weight_grad: float32 [2048, 5632], P('fs', 'tp')
- gate_taps_grad: float32 [3, 5632], P(None, 'tp')
- val_taps_grad: float32 [3, 5632], P(None, 'tp')
- gate_row_norms: float32 [2048], P('fs')
- val_row_norms: float32 [2048], P('fs')
- tap_row_norms: float32 [2, 3], replicated
All inputs are finite; a program needn't handle non-finite values.
Results may differ from a plain program's by a relative error of at most 0.017.
Values may be sent and summed in bfloat16 or wider, within the bound.
A program may use at most 128 MiB of HBM per device.

v0:
```python
import functools

import jax
import jax.numpy as jnp
from jax import lax
from jax.sharding import Mesh
from jax.sharding import PartitionSpec as P

SEQ = 1024
FS = ("fs_0", "fs_1")
FS_TP = ("fs_0", "fs_1", "tp")


def over_axes(value, axes):
    return functools.reduce(lax.psum, axes, value)


def sent_together(arrays, axis, dim, along):
    widths = [a.shape[along] for a in arrays]
    both = jnp.concatenate(arrays, axis=along)
    whole = lax.all_gather(both, axis, axis=dim, tiled=True)
    return tuple(jnp.split(whole, [sum(widths[:k]) for k in range(1, len(widths))], axis=along))


def cut_along(value, dim, size):
    before, after = (value.shape[:dim], value.shape[dim + 1 :])
    return jnp.moveaxis(value.reshape(*before, size, -1, *after), dim, 0)


def sum_at_owner(value, axis, dim):
    size = lax.axis_size(axis)
    pieces = lax.all_to_all(cut_along(value, dim, size), axis, 0, 0, tiled=True)
    return jnp.sum(pieces.astype(jnp.float32), axis=0)


def from_everyone(value, axis):
    size = lax.axis_size(axis)
    return lax.all_to_all(
        jnp.broadcast_to(value[None], (size, *value.shape)), axis, 0, 0, tiled=True
    )


def taken_together(value, axis):
    return from_everyone(value, axis).sum(axis=0)


def in_one(arrays, axis):
    ends = [0]
    for a in arrays:
        ends.append(ends[-1] + a.size)
    total = taken_together(jnp.concatenate([a.ravel() for a in arrays]), axis)
    return tuple((total[b:e].reshape(a.shape) for a, b, e in zip(arrays, ends, ends[1:])))


def shifted_sum(padded, kernel, length, backward):
    tap_count = kernel.shape[0]
    result = jnp.zeros((padded.shape[0], length, padded.shape[2]), jnp.float32)
    for tap_index in range(tap_count):
        tap_shift = tap_count - 1 - tap_index if backward else tap_index
        result = (
            result + kernel[tap_index][None, None, :] * padded[:, tap_shift : tap_shift + length]
        )
    return result


def local_grads(up_gate, up_val, hidden_grad, gate_taps, val_taps):
    length = up_gate.shape[1]
    tap_count = gate_taps.shape[0]
    gate_kernel = gate_taps.astype(jnp.float32)
    val_kernel = val_taps.astype(jnp.float32)
    pad_front = ((0, 0), (tap_count - 1, 0), (0, 0))
    pad_back = ((0, 0), (0, tap_count - 1), (0, 0))
    padded_gate = jnp.pad(up_gate.astype(jnp.float32), pad_front)
    padded_val = jnp.pad(up_val.astype(jnp.float32), pad_front)
    conv_gate = shifted_sum(padded_gate, gate_kernel, length, False)
    conv_val = shifted_sum(padded_val, val_kernel, length, False)
    sigmoid_gate = jax.nn.sigmoid(conv_gate)
    grad_hidden = hidden_grad.astype(jnp.float32)
    val_back = grad_hidden * conv_gate * sigmoid_gate
    gate_back = grad_hidden * conv_val * sigmoid_gate * (1.0 + conv_gate * (1.0 - sigmoid_gate))
    up_gate_back = shifted_sum(jnp.pad(gate_back, pad_back), gate_kernel, length, True).astype(
        jnp.bfloat16
    )
    up_val_back = shifted_sum(jnp.pad(val_back, pad_back), val_kernel, length, True).astype(
        jnp.bfloat16
    )
    tap_gate = jnp.stack(
        [
            jnp.sum(padded_gate[:, tap_index : tap_index + length] * gate_back, axis=(0, 1))
            for tap_index in range(tap_count)
        ]
    )
    tap_val = jnp.stack(
        [
            jnp.sum(padded_val[:, tap_index : tap_index + length] * val_back, axis=(0, 1))
            for tap_index in range(tap_count)
        ]
    )
    return (up_gate_back, up_val_back, tap_gate, tap_val)


def local(tokens, up_gate, up_val, gate_weight, val_weight, gate_taps, val_taps, hidden_grad):
    seq_count = up_gate.shape[0] // SEQ

    def as_blocks(values):
        return values.reshape(seq_count, SEQ, values.shape[1])

    gate_back, val_back, tap_gate, tap_val = local_grads(
        as_blocks(up_gate), as_blocks(up_val), as_blocks(hidden_grad), gate_taps, val_taps
    )
    gate_back = gate_back.reshape(up_gate.shape)
    val_back = val_back.reshape(up_val.shape)
    tap_gate, tap_val = (over_axes(tap_gate, FS), over_axes(tap_val, FS))
    token_rows = lax.all_gather(tokens, "tp", axis=0, tiled=True)
    weight_contract = (((0,), (0,)), ((), ()))

    def columns():
        return token_rows

    gate_summed = sum_at_owner(
        lax.dot_general(
            columns(), gate_back, weight_contract, preferred_element_type=jnp.float32
        ).astype(jnp.bfloat16),
        FS,
        0,
    )
    val_summed = sum_at_owner(
        lax.dot_general(
            columns(), val_back, weight_contract, preferred_element_type=jnp.float32
        ).astype(jnp.bfloat16),
        FS,
        0,
    )
    gate_whole, val_whole = sent_together((gate_weight, val_weight), FS, 0, 1)
    contract = (((1,), (1,)), ((), ()))
    total = lax.dot_general(gate_back, gate_whole, contract, preferred_element_type=jnp.float32)
    input_grad = lax.psum_scatter(
        (
            total
            + lax.dot_general(val_back, val_whole, contract, preferred_element_type=jnp.float32)
        ).astype(jnp.bfloat16),
        "tp",
        scatter_dimension=0,
        tiled=True,
    )
    tap_squares = jnp.stack(
        [jnp.sum(tap_gate * tap_gate, axis=1), jnp.sum(tap_val * tap_val, axis=1)]
    )
    gate_norms, val_norms, tap_norms = in_one(
        (
            jnp.sum(gate_summed * gate_summed, axis=1),
            jnp.sum(val_summed * val_summed, axis=1),
            tap_squares,
        ),
        "tp",
    )
    return (
        input_grad,
        gate_summed,
        val_summed,
        tap_gate,
        tap_val,
        gate_norms,
        val_norms,
        tap_norms,
    )


def solution(mesh):
    split = Mesh(mesh.devices.reshape(4, 4, mesh.shape["tp"]), ("fs_0", "fs_1", "tp"))
    in_specs = (
        P(FS_TP, None),
        P(FS, "tp"),
        P(FS, "tp"),
        P(FS, "tp"),
        P(FS, "tp"),
        P(None, "tp"),
        P(None, "tp"),
        P(FS, "tp"),
    )
    out_specs = (
        P(FS_TP, None),
        P(FS, "tp"),
        P(FS, "tp"),
        P(None, "tp"),
        P(None, "tp"),
        P(FS),
        P(FS),
        P(),
    )
    return jax.shard_map(local, mesh=split, in_specs=in_specs, out_specs=out_specs, check_vma=False)
```

profile of v0, /device:TPU:1, one launch (start us, length us, event | category | flops | bytes accessed | tf_op | source)
XLA Modules:
  0.0 234.5 jit_solution(10474045750977695871)
XLA Ops:
  7.2 0.0 all-gather.3.cloned.1.call-start
  7.2 1.6 pad_maximum_fusion
  8.8 0.0 all-gather.3.cloned.1.call-update
  8.9 0.0 all-gather.5.cloned.1.call-start
  8.9 0.7 all-gather.5.cloned.1.call-update
  9.6 0.0 reduce-scatter.2.cloned.1.call-start
  9.7 0.7 convert_element_type.57
  10.3 0.7 convert_element_type.60
  11.0 3.8 %reshape.63 = f32[2,1024,352]{1,0,2:T(2,128)S(1)} reshape(bf16[2048,352]{0,1:T(8,128)(2,1)} %param.9) | data formatting | bytes 4325376 | tf_op jit(solution)/shard_map/convert_element_type | solution.py:73
  14.8 5.0 %reshape.62 = f32[2,1024,352]{1,0,2:T(2,128)} reshape(bf16[2048,352]{0,1:T(8,128)(2,1)} %param.10) | data formatting | bytes 4325376 | tf_op jit(solution)/shard_map/convert_element_type | solution.py:74
  19.8 5.0 %reshape.61 = f32[2,1024,352]{1,0,2:T(2,128)} reshape(bf16[2048,352]{0,1:T(8,128)(2,1)} %param.15) | data formatting | bytes 4325376 | tf_op jit(solution)/shard_map/convert_element_type | solution.py:78
  24.8 0.0 copy-start
  24.8 0.0 copy-start.1
  24.8 25.5 %multiply_reduce_fusion.2 = (f32[352]{0:T(512)S(1)}, f32[352]{0:T(512)S(1)}, f32[352]{0:T(512)S(1)}, f32[2,1024,352]{1,0,2:T(2,128)S(1)}, f32[2,1024,352]{1,0,2:T(2,128)S(1)}) fusion(f32[2,1024,352]{1,0,2:T(2,128)} %reshape.62, f32[2,1024,352]{1,0,2:T(2,128)} %reshape.61, f32[2,1024,352]{1,0,2:T(2,128)S(1)} %reshape.63, f32[352]{0:T(512)S(1)} %get-tuple-element.18, ...), kind=kLoop, calls=%fused_computation.3 | loop fusion | flops 11533280 | bytes 14426368 | tf_op jit(solution)/shard_map/reduce_sum | solution.py:95
  50.4 0.0 copy-done
  50.4 0.0 copy-done.1
  50.4 30.8 %multiply_reduce_fusion.5 = (f32[352]{0:T(512)S(1)}, f32[352]{0:T(512)S(1)}, f32[352]{0:T(512)S(1)}, f32[2,1024,352]{1,0,2:T(2,128)S(1)}, bf16[2,1024,352]{1,0,2:T(2,128)(2,1)S(1)}) fusion(f32[2,1024,352]{1,0,2:T(2,128)S(1)} %reshape.63, f32[2,1024,352]{1,0,2:T(2,128)S(1)} %get-tuple-element.25, f32[2,1024,352]{1,0,2:T(2,128)S(1)} %copy-done.1, ...), kind=kLoop, calls=%fused_computation.6 | loop fusion | flops 18742240 | bytes 18751744 | tf_op jit(solution)/shard_map/reduce_sum | solution.py:89
  81.2 8.7 %add_convert_fusion.2 = bf16[2,1024,352]{1,0,2:T(2,128)(2,1)S(1)} fusion(f32[2,1024,352]{1,0,2:T(2,128)S(1)} %get-tuple-element.26, f32[352]{0:T(512)S(1)} %get-tuple-element.18, f32[352]{0:T(512)S(1)} %get-tuple-element.19, f32[352]{0:T(512)S(1)} %get-tuple-element.17), kind=kLoop, calls=%fused_computation.11 | loop fusion | flops 4325376 | bytes 4329600 | tf_op jit(solution)/shard_map/convert_element_type | solution.py:81
  89.9 0.4 copy.29
  90.3 0.4 copy.30
  90.7 0.0 all-gather.3.cloned.1.call-done
  90.7 0.0 copy-start.2
  90.7 10.0 %fusion.3 = f32[2048,2048]{1,0:T(8,128)} fusion(bf16[2048,352]{0,1:T(8,128)(2,1)S(1)} %bitcast.36, bf16[2048,704]{0,1:T(8,128)(2,1)} %all-gather.3.cloned.1.call-done), kind=kOutput, calls=%fused_computation.26 | convolution fusion | flops 2952790016 | bytes 19660800 | tf_op jit(solution)/shard_map/dot_general | solution.py:136
  100.8 0.0 copy-done.2
  100.8 10.5 %add_convert_fusion = bf16[2048,2048]{1,0:T(8,128)(2,1)} fusion(f32[2048,2048]{1,0:T(8,128)} %fusion.3, bf16[2048,352]{0,1:T(8,128)(2,1)S(1)} %bitcast.34, bf16[2048,704]{0,1:T(8,128)(2,1)S(1)} %copy-done.2), kind=kOutput, calls=%fused_computation | convolution fusion | flops 2961178624 | bytes 28049408 | tf_op jit(solution)/shard_map/dot_general | solution.py:140
  111.3 0.0 reduce-scatter.2.cloned.1.call-update
  111.3 16.6 %all-gather.5.cloned.1.call-done = bf16[2048,2048]{1,0:T(8,128)(2,1)} async-done(((bf16[128,2048]{1,0:T(8,128)(2,1)}), bf16[2048,2048]{1,0:T(8,128)(2,1)}) %all-gather.5.cloned.1.call-update) | async-done | bytes 8388624 | tf_op jit(solution)/shard_map/all_gather | solution.py:114
  127.9 6.5 %fusion = bf16[44,16,8,128]{3,2,1,0:T(8,128)(2,1)S(1)} fusion(bf16[2048,352]{0,1:T(8,128)(2,1)S(1)} %bitcast.37, bf16[2048,2048]{1,0:T(8,128)(2,1)} %all-gather.5.cloned.1.call-done), kind=kOutput, calls=%fused_computation.21 | convolution fusion | flops 2953510912 | bytes 11272192 | tf_op jit(solution)/shard_map/dot_general | solution.py:121
  134.4 1.4 copy.34
  135.8 6.5 %all-to-all-start = ((bf16[16,128,352]{1,2,0:T(8,128)(2,1)}), bf16[16,128,352]{1,2,0:T(8,128)(2,1)S(1)}, u32[]{:S(2)}, u32[]{:S(2)}) async-start(bf16[16,128,352]{1,2,0:T(8,128)(2,1)} %bitcast.38), calls=%async_computation.1 | async-start | bytes 2883584 | tf_op jit(solution)/shard_map/all_to_all | solution.py:32
  142.3 6.6 %fusion.1 = bf16[44,16,8,128]{3,2,1,0:T(8,128)(2,1)S(1)} fusion(bf16[2048,352]{0,1:T(8,128)(2,1)S(1)} %bitcast.35, bf16[2048,2048]{1,0:T(8,128)(2,1)} %all-gather.5.cloned.1.call-done), kind=kOutput, calls=%fused_computation.22 | convolution fusion | flops 2953510912 | bytes 11272192 | tf_op jit(solution)/shard_map/dot_general | solution.py:128
  148.9 1.4 copy.33
  150.3 14.4 %all-to-all-done = bf16[16,128,352]{1,2,0:T(8,128)(2,1)S(1)} async-done(((bf16[16,128,352]{1,2,0:T(8,128)(2,1)}), bf16[16,128,352]{1,2,0:T(8,128)(2,1)S(1)}, u32[]{:S(2)}, u32[]{:S(2)}) %all-to-all-start) | async-done | bytes 1441824 | tf_op jit(solution)/shard_map/all_to_all | solution.py:32
  164.7 4.1 %all-to-all-start.1 = ((bf16[16,128,352]{1,2,0:T(8,128)(2,1)}), bf16[16,128,352]{1,2,0:T(8,128)(2,1)S(1)}, u32[]{:S(2)}, u32[]{:S(2)}) async-start(bf16[16,128,352]{1,2,0:T(8,128)(2,1)} %bitcast.32), calls=%async_computation.2 | async-start | bytes 2883584 | tf_op jit(solution)/shard_map/all_to_all | solution.py:32
  168.9 23.1 %all-reduce.5 = (f32[3,352]{1,0:T(4,128)S(1)}, f32[3,352]{1,0:T(4,128)S(1)}) all-reduce(f32[3,352]{1,0:T(4,128)S(1)} %get-tuple-element.30, f32[3,352]{1,0:T(4,128)S(1)} %get-tuple-element.31), channel_id=1, replica_groups=mesh['fs_0'=4,'fs_1'=4,'tp'=16] {'fs_0'}, use_global_device_ids=true, to_apply=%region_6.7 | all-reduce | flops 2112 | bytes 16896 | tf_op jit(solution)/shard_map/psum | solution.py:15
  191.9 15.9 %all-reduce.4 = (f32[3,352]{1,0:T(4,128)S(1)}, f32[3,352]{1,0:T(4,128)S(1)}) all-reduce(f32[3,352]{1,0:T(4,128)S(1)} %get-tuple-element.22, f32[3,352]{1,0:T(4,128)S(1)} %get-tuple-element.23), channel_id=1, replica_groups=mesh['fs_0'=4,'fs_1'=4,'tp'=16] {'fs_1'}, use_global_device_ids=true, to_apply=%region_7.8 | all-reduce | flops 2112 | bytes 16896 | tf_op jit(solution)/shard_map/psum | solution.py:15
  207.9 0.0 copy-start.5
  207.9 0.0 copy-start.6
  207.9 0.1 multiply_reduce_fusion.9
  208.0 0.1 multiply_reduce_fusion.8
  208.1 0.1 reshape.59
  208.2 0.2 convert_reduce_fusion.1
  208.4 0.0 copy-start.3
  208.4 0.1 multiply_reduce_fusion.7
  208.5 0.0 all-to-all-done.1
  208.5 0.2 convert_reduce_fusion
  208.7 0.0 copy-start.4
  208.7 0.1 multiply_reduce_fusion.6
  208.8 17.9 %all_to_all.16 = f32[16,1,262]{2,1,0:T(1,128)S(1)} all-to-all(f32[16,1,262]{2,1,0:T(1,128)S(1)} %broadcast_in_dim.2), channel_id=1, replica_groups=mesh['fs_0'=4,'fs_1'=4,'tp'=16] {'tp'}, dimensions={0} | all-to-all | bytes 33536 | tf_op jit(solution)/shard_map/all_to_all | solution.py:38
  226.8 0.6 reshape.60
  227.4 0.5 fusion.5
  227.9 0.0 reduce-scatter.2.cloned.1.call-done
  227.9 0.0 copy-done.5
  227.9 0.0 copy-done.6
  228.0 0.0 copy-done.3
  228.0 0.0 copy-done.4
  (14 shorter events, 0.2 us)
Async XLA Ops:
  7.2 83.6 %all-gather.3.cloned.1.call-start = ((), (), s32[]{:S(2)}) async-start(), calls=%async_computation.4 | async-start | bytes 3063808 | tf_op jit(solution)/shard_map/all_gather | solution.py:21
  8.9 119.0 %all-gather.5.cloned.1.call-start = ((), (), s32[]{:S(2)}) async-start(), calls=%async_computation.6 | async-start | bytes 8912896 | tf_op jit(solution)/shard_map/all_gather | solution.py:114
  9.6 218.3 %reduce-scatter.2.cloned.1.call-start = ((), (), s32[]{:S(2)}) async-start(), calls=%async_computation.5 | async-start | bytes 8912896 | tf_op jit(solution)/shard_map/reduce_scatter | solution.py:137
  24.8 25.6 %copy-start = (f32[2,1024,352]{1,0,2:T(2,128)S(1)}, f32[2,1024,352]{1,0,2:T(2,128)}, u32[]{:S(2)}) copy-start(f32[2,1024,352]{1,0,2:T(2,128)} %reshape.62) | copy-start | bytes 8650756
  24.8 25.6 %copy-start.1 = (f32[2,1024,352]{1,0,2:T(2,128)S(1)}, f32[2,1024,352]{1,0,2:T(2,128)}, u32[]{:S(2)}) copy-start(f32[2,1024,352]{1,0,2:T(2,128)} %reshape.61) | copy-start | bytes 8650756
  90.7 10.0 %copy-start.2 = (bf16[2048,704]{0,1:T(8,128)(2,1)S(1)}, bf16[2048,704]{0,1:T(8,128)(2,1)}, u32[]{:S(2)}) copy-start(bf16[2048,704]{0,1:T(8,128)(2,1)} %all-gather.3.cloned.1.call-done) | copy-start | bytes 8650756
  135.8 28.9 %all-to-all-start = ((bf16[16,128,352]{1,2,0:T(8,128)(2,1)}), bf16[16,128,352]{1,2,0:T(8,128)(2,1)S(1)}, u32[]{:S(2)}, u32[]{:S(2)}) async-start(bf16[16,128,352]{1,2,0:T(8,128)(2,1)} %bitcast.38), calls=%async_computation.1 | async-start | bytes 2883584 | tf_op jit(solution)/shard_map/all_to_all | solution.py:32
  164.7 43.8 %all-to-all-start.1 = ((bf16[16,128,352]{1,2,0:T(8,128)(2,1)}), bf16[16,128,352]{1,2,0:T(8,128)(2,1)S(1)}, u32[]{:S(2)}, u32[]{:S(2)}) async-start(bf16[16,128,352]{1,2,0:T(8,128)(2,1)} %bitcast.32), calls=%async_computation.2 | async-start | bytes 2883584 | tf_op jit(solution)/shard_map/all_to_all | solution.py:32
  207.9 20.1 %copy-start.5 = (f32[3,352]{1,0:T(4,128)}, f32[3,352]{1,0:T(4,128)S(1)}, u32[]{:S(2)}) copy-start(f32[3,352]{1,0:T(4,128)S(1)} %get-tuple-element.20) | copy-start | bytes 12676
  207.9 20.1 %copy-start.6 = (f32[3,352]{1,0:T(4,128)}, f32[3,352]{1,0:T(4,128)S(1)}, u32[]{:S(2)}) copy-start(f32[3,352]{1,0:T(4,128)S(1)} %get-tuple-element.21) | copy-start | bytes 12676
  208.4 19.5 %copy-start.3 = (f32[128,352]{0,1:T(8,128)}, f32[128,352]{0,1:T(8,128)S(1)}, u32[]{:S(2)}) copy-start(f32[128,352]{0,1:T(8,128)S(1)} %convert_reduce_fusion.1) | copy-start | bytes 540676
  208.7 19.3 %copy-start.4 = (f32[128,352]{0,1:T(8,128)}, f32[128,352]{0,1:T(8,128)S(1)}, u32[]{:S(2)}) copy-start(f32[128,352]{0,1:T(8,128)S(1)} %convert_reduce_fusion) | copy-start | bytes 540676
Sparse Core Ops, SparseCore 0:
  11.0 58.0 all-gather.2
  70.8 57.0 all-gather.4
  131.0 67.2 reduce-scatter.1
where the time goes:
time: 235 us
  other arithmetic  68.9 us (29%)
  blocking collectives  56.9 us (24%)
  matrix products  33.7 us (14%)
  waiting for transfers between devices  31.8 us (14%)
  local copies, waits for them, and re-layouts  18.6 us (8%)
  between operations  14 us (6%)
  starting transfers between devices  10.7 us (5%)
    psum x2, blocking collectives, over_axes(): return functools.reduce(lax.psum, axes, value)  39 us
    reduce_sum x1, other arithmetic, local_grads(): jnp.sum(padded_gate[:, tap_index:tap_index + length] * gate_back, axis=(0...  30.8 us
    reduce_sum x1, other arithmetic, local_grads(): jnp.sum(padded_val[:, tap_index:tap_index + length] * val_back, axis=(0, 1))  25.5 us
    all_to_all x1, blocking collectives, from_everyone(): lax.all_to_all(jnp.broadcast_to(value[None], (size, *value.shape)), axis,...  17.9 us
    all_gather x1, waiting for transfers between devices, local(): token_rows = lax.all_gather(tokens, 'tp', axis=0, tiled=True)  16.6 us
    all_to_all x2, waiting for transfers between devices, sum_at_owner(): pieces = lax.all_to_all(cut_along(value, dim, size), axis, 0, 0, tiled=True)  14.4 us
    all_to_all x2, starting transfers between devices, sum_at_owner(): pieces = lax.all_to_all(cut_along(value, dim, size), axis, 0, 0, tiled=True)  10.6 us
    dot_general x1, matrix products, local(): lax.dot_general(val_back, val_whole, contract, preferred_element_type=jnp...  10.5 us
  transfers between devices with their start and end apart: 5, of which 2 were waited for; matrix products, arithmetic and copies ran while one was open for 51% of the time, Pallas kernels for 0%

commit v1 on v0

v1 whole, which is shorter than its diff:
```python
import itertools

import jax
import jax.numpy as jnp
from jax import lax
from jax.experimental import pallas as pl
from jax.experimental.pallas import tpu as pltpu
from jax.sharding import Mesh
from jax.sharding import PartitionSpec as P

F32, BF16 = jnp.float32, jnp.bfloat16
MESH = pl.DeviceIdType.MESH
SEQ = 1024
D = 2048
ROWS = 128
WIDTH = 352
WIDE = 384
PAD = 16
CHUNK = 64
NT = (((1,), (1,)), ((), ()))
NN = (((1,), (0,)), ((), ()))
N_COPIES = 106


def kernel(
    tok, ug, uv, gw, vw, gt, vt, hg,
    ig_o, gwg_o, vwg_o, gtg_o, vtg_o, gn_o, vn_o, tn_o,
    TOK, UGI, UVI, HGI, WT, UB, UBT, W, ACC, DA, DB, DA2, DB2,
    RA0, RA1, RB0, RB1, SA0, SA1, SB0, SB1, PB, PX, RS, TX, TY, NC, NZ,
    lsem, ssem, rsem,
):
    y, x, z, c = (lax.axis_index(a) for a in ("y", "x", "z", "c"))
    p = 1 - c

    def ahead(i, k, n):
        return lax.rem(i + k, n)

    ids = itertools.count()
    started = []

    def remote(src, dst, **dev):
        i = next(ids)
        copy = pltpu.make_async_remote_copy(
            src_ref=src, dst_ref=dst, send_sem=ssem.at[i], recv_sem=rsem.at[i],
            device_id=dev, device_id_type=MESH,
        )
        copy.start()
        started.append(copy)
        return copy

    def load(src, dst, i):
        copy = pltpu.make_async_copy(src, dst, lsem.at[i])
        copy.start()
        return copy

    own_rows = pl.ds(pl.multiple_of(c * ROWS, ROWS), ROWS)
    l_tok = load(tok, TOK.at[z, own_rows], 0)
    l_gw = load(gw, WT.at[0], 1)
    l_vw = load(vw, WT.at[1], 2)
    l_in = []
    for s in range(2):
        at = pl.ds(s * SEQ, SEQ)
        l_in.append(
            (
                load(ug.at[at], UGI.at[s, pl.ds(PAD, SEQ)], 3 + 3 * s),
                load(uv.at[at], UVI.at[s, pl.ds(PAD, SEQ)], 4 + 3 * s),
                load(hg.at[at], HGI.at[s], 5 + 3 * s),
            )
        )

    barrier = pltpu.get_barrier_semaphore()
    peers = [{"c": p}]
    peers += [{"x": ahead(x, k, 4)} for k in (1, 2, 3)]
    peers += [{"y": ahead(y, k, 4)} for k in (1, 2, 3)]
    peers += [{"z": ahead(z, k, 8)} for k in range(1, 8)]
    for peer in peers:
        pl.semaphore_signal(barrier, inc=1, device_id=peer, device_id_type=MESH)

    l_gw.wait()
    l_vw.wait()
    W[y, x] = jnp.zeros((ROWS, 2 * WIDE), BF16)
    W[y, x, :, 0:WIDTH] = WT[0]
    W[y, x, :, WIDE : WIDE + WIDTH] = WT[1]
    l_tok.wait()
    pl.semaphore_wait(barrier, len(peers))

    def tok_at(zz, core, h):
        return TOK.at[zz, pl.ds(pl.multiple_of(core * ROWS + h * 64, 64), 64)]

    order_up = [(0, 0), (0, 1), (1, 0), (1, 1), (2, 0), (2, 1), (3, 0)]
    order_dn = [(s, 1 - h) for s, h in order_up]
    up, down, cross = {}, {}, {}

    def tok_send(j):
        s, h = order_up[j]
        blk = tok_at(ahead(z, 8 - s, 8), c, h)
        up[j] = remote(blk, blk, z=ahead(z, 1, 8))
        s, h = order_dn[j]
        blk = tok_at(ahead(z, s, 8), c, h)
        down[j] = remote(blk, blk, z=ahead(z, 7, 8))

    def tok_cross(k, h):
        blk = tok_at(ahead(z, k, 8), c, h)
        cross[k, h] = remote(blk, blk, c=p)

    def tok_event(j):
        up[j].wait_recv()
        down[j].wait_recv()
        if j + 2 < 7:
            tok_send(j + 2)
        s, h = order_up[j]
        tok_cross(7 - s, h)
        s, h = order_dn[j]
        tok_cross(1 + s, h)

    tok_send(0)
    tok_send(1)
    tok_cross(0, 0)
    tok_cross(0, 1)

    def gather(slot, axis, i):
        state = {}

        def begin():
            for d, s in ((0, 1), (1, 3)):
                state[d] = remote(slot(i, None), slot(i, None), **{axis: ahead(i, s, 4)})

        def middle():
            for d, s in ((0, 1), (1, 3)):
                state[d].wait_recv()
                far = ahead(i, 4 - s, 4)
                state[2 + d] = remote(slot(far, d), slot(far, d), **{axis: ahead(i, s, 4)})

        def end():
            state[2].wait_recv()
            state[3].wait_recv()

        return begin, middle, end

    def a1(i, d):
        return W.at[y, i, pl.ds(0, 64) if d is None else pl.ds(32 * d, 32)]

    def b1(i, d):
        return W.at[i, x, pl.ds(64, 64) if d is None else pl.ds(64 + 32 * d, 32)]

    def a2(i, d):
        return W.at[i, pl.ds(0, 4) if d is None else pl.ds(2 * d, 2), pl.ds(0, 64)]

    def b2(i, d):
        return W.at[pl.ds(0, 4) if d is None else pl.ds(2 * d, 2), i, pl.ds(64, 64)]

    first = gather(a1, "x", x), gather(b1, "y", y)
    second = gather(a2, "y", y), gather(b2, "x", x)
    for g in first:
        g[0]()

    for s in range(2):
        UGI[s, 0:PAD] = jnp.zeros((PAD, WIDTH), BF16)
        UVI[s, 0:PAD] = jnp.zeros((PAD, WIDTH), BF16)
    UB[:, 256:384] = jnp.zeros((2 * SEQ, 128), BF16)
    UB[:, 640:768] = jnp.zeros((2 * SEQ, 128), BF16)
    TX[x] = jnp.zeros((2, 8, WIDE), F32)

    def conv(s, t):
        lo, hi = t * 128, min(t * 128 + 128, WIDTH)
        n = hi - lo
        kg = [gt[i : i + 1, lo:hi].astype(F32) for i in range(3)]
        kv = [vt[i : i + 1, lo:hi].astype(F32) for i in range(3)]

        def fold(a):
            return jnp.sum(a.reshape(CHUNK // 8, 8, n), axis=0)

        def step(j, carry):
            sums, gb_next, vb_next = carry
            r = pl.multiple_of((SEQ // CHUNK - 1 - j) * CHUNK, CHUNK)
            g = UGI[s, pl.ds(r, CHUNK + PAD), lo:hi].astype(F32)
            v = UVI[s, pl.ds(r, CHUNK + PAD), lo:hi].astype(F32)
            h = HGI[s, pl.ds(r, CHUNK), lo:hi].astype(F32)
            gs = [g[PAD - 2 + i : PAD - 2 + i + CHUNK] for i in range(3)]
            vs = [v[PAD - 2 + i : PAD - 2 + i + CHUNK] for i in range(3)]
            cg = kg[0] * gs[0] + kg[1] * gs[1] + kg[2] * gs[2]
            cv = kv[0] * vs[0] + kv[1] * vs[1] + kv[2] * vs[2]
            sg = jax.nn.sigmoid(cg)
            hs = h * sg
            vb = hs * cg
            gb = hs * cv * (1.0 + cg * (1.0 - sg))
            sums = tuple(
                a + fold(b)
                for a, b in zip(sums, [u * gb for u in gs] + [u * vb for u in vs])
            )
            gx = jnp.concatenate([gb, gb_next], axis=0)
            vx = jnp.concatenate([vb, vb_next], axis=0)
            og = kg[2] * gb + kg[1] * gx[1 : CHUNK + 1] + kg[0] * gx[2 : CHUNK + 2]
            ov = kv[2] * vb + kv[1] * vx[1 : CHUNK + 1] + kv[0] * vx[2 : CHUNK + 2]
            at = pl.ds(s * SEQ + r, CHUNK)
            UB[at, lo:hi] = og.astype(BF16)
            UB[at, WIDE + lo : WIDE + hi] = ov.astype(BF16)
            return sums, gb[0:8], vb[0:8]

        zero = jnp.zeros((8, n), F32)
        sums, _, _ = lax.fori_loop(0, SEQ // CHUNK, step, ((zero,) * 6, zero, zero))
        for i in range(3):
            for q in range(2):
                TX[x, q, i : i + 1, lo:hi] += jnp.sum(sums[3 * q + i], axis=0, keepdims=True)

    def turn(zz):
        for t in range(6):
            UBT[zz, t * 128 : t * 128 + 128, :] = UB[
                pl.ds(pl.multiple_of(zz * 256, 256), 256), t * 128 : t * 128 + 128
            ].T

    def weight_part(ks, first_part=False, last_part=False):
        zs = [ahead(z, k, 8) for k in ks]

        def step(n, _):
            cols = pl.ds(pl.multiple_of(n * 256, 256), 256)
            total = None
            for zz in zs:
                part = lax.dot_general(UBT[zz], TOK[zz, :, cols], NN, preferred_element_type=F32)
                total = part if total is None else total + part
            if not first_part:
                total = total + ACC[n]
            if last_part:
                out = total.astype(BF16)
                yy, xx = n // 2, 2 * (n % 2)
                for q in range(2):
                    DA[xx + q, yy // 2, yy % 2] = out[0:WIDE, q * 128 : q * 128 + 128]
                    DB[yy, xx // 2, q] = out[WIDE : 2 * WIDE, q * 128 : q * 128 + 128]
            else:
                ACC[n] = total
            return 0

        lax.fori_loop(0, 8, step, 0)

    def wait_cross(*ks):
        for k in ks:
            cross[k, 0].wait_recv()
            cross[k, 1].wait_recv()

    partner = {}

    def input_part(k):
        zz = ahead(z, k, 8)
        rows = pl.ds(pl.multiple_of(zz * 256, 256), 256)

        def step(n, _):
            w = W[n // 2, pl.ds(2 * (n % 2), 2)].reshape(256, 2 * WIDE)
            out = lax.dot_general(UB[rows, :], w, NT, preferred_element_type=F32).astype(BF16)
            cols = pl.ds(pl.multiple_of(n * 256, 256), 256)
            PB[k, 0, :, cols] = out[0:128]
            PB[k, 1, :, cols] = out[128:256]
            return 0

        lax.fori_loop(0, 8, step, 0)
        partner[k] = remote(PB.at[k, p], PX.at[k], c=p)

    sum_up = [(0, 0), (1, 1), (1, 0), (2, 1), (2, 0), (3, 1), (3, 0)]
    flow = {}

    def pair_sum(k, h, extra):
        def step(i, _):
            rows = pl.ds(pl.multiple_of(h * 64 + i * 16, 16), 16)
            v = PB[k, c, rows, :].astype(F32) + PX[k, rows, :].astype(F32)
            if extra is not None:
                v = v + RS[extra[0], extra[1], pl.ds(pl.multiple_of(i * 16, 16), 16), :].astype(F32)
            PB[k, c, rows, :] = v.astype(BF16)
            return 0

        lax.fori_loop(0, 4, step, 0)

    def sum_event(j):
        for d in range(2):
            s, h = sum_up[j]
            if d:
                h = 1 - h
            k = 4 - s if d == 0 else 4 + s
            if j == 0 and d == 0 or j == 1 or j == 3 or j == 5:
                partner[k].wait_recv()
            if j >= 2:
                flow[d, j - 2].wait_recv()
            pair_sum(k, h, (d, j - 2) if j >= 2 else None)
            flow[d, j] = remote(
                PB.at[k, c, pl.ds(h * 64, 64)], RS.at[d, j], z=ahead(z, 1 if d == 0 else 7, 8)
            )

    def scatter(src, r0, r1, axis, i):
        state = {}
        own = i
        near = {0: ahead(i, 1, 4), 1: ahead(i, 3, 4)}
        far = ahead(i, 2, 4)

        def begin():
            for d in range(2):
                to = {axis: near[d]}
                state[d] = remote(src.at[far, d], r0.at[d], **to)
                state[2 + d] = remote(src.at[near[d], 1 - d], r1.at[d, 1 - d], **to)

        def middle():
            for d in range(2):
                state[d].wait_recv()
                src[near[d], d] = (src[near[d], d].astype(F32) + r0[d].astype(F32)).astype(BF16)
                state[4 + d] = remote(src.at[near[d], d], r1.at[d, d], **{axis: near[d]})

        def end():
            for i_ in range(2, 6):
                state[i_].wait_recv()

        def total(*at):
            t = src[(own, *at)].astype(F32)
            return t + r1[(0, *at)].astype(F32) + r1[(1, *at)].astype(F32)

        return begin, middle, end, total

    sc_a1 = scatter(DA, RA0, RA1, "x", x)
    sc_b1 = scatter(DB, RB0, RB1, "y", y)
    sc_a2 = scatter(DA2, SA0, SA1, "y", y)
    sc_b2 = scatter(DB2, SB0, SB1, "x", x)

    def tap_sum(ref):
        return ref[0] + ref[1] + ref[2] + ref[3]

    for s in range(2):
        for copy in l_in[s]:
            copy.wait()
        for t in range(3):
            conv(s, t)
            if s == 0 and t == 1:
                for g in first:
                    g[1]()
            if s == 1 and t == 0:
                for g in first:
                    g[2]()
                for g in second:
                    g[0]()
    tap_x = [remote(TX.at[x], TX.at[x], x=ahead(x, k, 4)) for k in (1, 2, 3)]
    tok_event(0)
    lax.fori_loop(0, 8, lambda i, _: (turn(i), 0)[1], 0)
    tok_event(1)
    for copy in tap_x:
        copy.wait_recv()
    TY[y] = tap_sum(TX)
    tap_y = [remote(TY.at[y], TY.at[y], y=ahead(y, k, 4)) for k in (1, 2, 3)]
    wait_cross(0)
    weight_part([0], first_part=True)
    tok_event(2)
    for g in second:
        g[1]()
    wait_cross(1, 7)
    weight_part([1, 7])
    tok_event(3)
    for copy in tap_y:
        copy.wait_recv()
    taps = tap_sum(TY)
    gtg_o[...] = taps[0, 0:3, 0:WIDTH]
    vtg_o[...] = taps[1, 0:3, 0:WIDTH]
    NC[c, 1] = jnp.broadcast_to(jnp.sum(taps[0] * taps[0], axis=1, keepdims=True), (8, 128))
    NC[c, 2] = jnp.broadcast_to(jnp.sum(taps[1] * taps[1], axis=1, keepdims=True), (8, 128))
    tok_event(4)
    for g in second:
        g[2]()
    input_part(4)
    input_part(3)
    input_part(5)
    tok_event(5)
    sum_event(0)
    sum_event(1)
    wait_cross(2, 6)
    weight_part([2, 6])
    tok_event(6)
    wait_cross(3, 5)
    weight_part([3, 5])
    wait_cross(4)
    weight_part([4], last_part=True)
    sc_a1[0]()
    sc_b1[0]()
    input_part(2)
    input_part(6)
    sum_event(2)
    input_part(1)
    sum_event(3)
    sc_a1[1]()
    sc_b1[1]()
    input_part(7)
    sum_event(4)
    input_part(0)
    sc_a1[2]()
    sc_b1[2]()
    for q in range(4):
        DA2[q] = sc_a1[3](q // 2, q % 2).astype(BF16).reshape(2, 192, 128)
        DB2[q] = sc_b1[3](q // 2, q % 2).astype(BF16).reshape(2, 192, 128)
    sc_a2[0]()
    sc_b2[0]()
    sum_event(5)
    sc_a2[1]()
    sc_b2[1]()
    sum_event(6)
    sc_a2[2]()
    sc_b2[2]()
    norms = []
    for scat, out in ((sc_a2, gwg_o), (sc_b2, vwg_o)):
        grad = scat[3]().reshape(WIDE, 128)
        norms.append(jnp.sum(grad * grad, axis=0, keepdims=True))
        out[...] = grad.T[:, 0:WIDTH]
    NC[c, 0, 0:1] = norms[0]
    NC[c, 0, 1:2] = norms[1]
    pair = remote(NC.at[c], NC.at[c], c=p)
    pair.wait_recv()
    NZ[z] = NC[0] + NC[1]
    along = [remote(NZ.at[z], NZ.at[z], z=ahead(z, k, 8)) for k in range(1, 8)]
    partner[0].wait_recv()
    for d in range(2):
        flow[d, 5].wait_recv()
        flow[d, 6].wait_recv()

    for h in range(2):
        j_up = 6 if h == 0 else 5
        j_dn = 5 if h == 0 else 6

        def step(i, _, h=h, j_up=j_up, j_dn=j_dn):
            rows = pl.ds(pl.multiple_of(h * 64 + i * 16, 16), 16)
            here = pl.ds(pl.multiple_of(i * 16, 16), 16)
            v = PB[0, c, rows, :].astype(F32) + PX[0, rows, :].astype(F32)
            v = v + RS[0, j_up, here, :].astype(F32) + RS[1, j_dn, here, :].astype(F32)
            ig_o[rows, :] = v.astype(BF16)
            return 0

        lax.fori_loop(0, 4, step, 0)

    for copy in along:
        copy.wait_recv()
    total = NZ[0]
    for k in range(1, 8):
        total = total + NZ[k]
    gn_o[...] = total[0, 0:1]
    vn_o[...] = total[0, 1:2]
    diagonal = lax.broadcasted_iota(jnp.int32, (8, 128), 0) == lax.broadcasted_iota(
        jnp.int32, (8, 128), 1
    )
    for q in range(2):
        row = jnp.sum(jnp.where(diagonal, total[1 + q], 0.0), axis=0, keepdims=True)
        tn_o[q : q + 1, :] = row[:, 0:3]
    for copy in started:
        copy.wait_send()
    assert len(started) == N_COPIES, len(started)


def local(tokens, up_gate, up_val, gate_weight, val_weight, gate_taps, val_taps, hidden_grad):
    hbm = pl.BlockSpec(memory_space=pl.ANY)
    vmem = pl.BlockSpec(memory_space=pltpu.VMEM)
    half = WIDE // 2
    scratch = [
        pltpu.VMEM((8, 256, D), BF16),
        pltpu.VMEM((2, PAD + SEQ, WIDTH), BF16),
        pltpu.VMEM((2, PAD + SEQ, WIDTH), BF16),
        pltpu.VMEM((2, SEQ, WIDTH), BF16),
        pltpu.VMEM((2, ROWS, WIDTH), BF16),
        pltpu.VMEM((2 * SEQ, 2 * WIDE), BF16),
        pltpu.VMEM((8, 2 * WIDE, 256), BF16),
        pltpu.VMEM((4, 4, ROWS, 2 * WIDE), BF16),
        pltpu.VMEM((8, 2 * WIDE, 256), F32),
        pltpu.VMEM((4, 2, 2, WIDE, 128), BF16),
        pltpu.VMEM((4, 2, 2, WIDE, 128), BF16),
        pltpu.VMEM((4, 2, half, 128), BF16),
        pltpu.VMEM((4, 2, half, 128), BF16),
        pltpu.VMEM((2, 2, WIDE, 128), BF16),
        pltpu.VMEM((2, 2, 2, WIDE, 128), BF16),
        pltpu.VMEM((2, 2, WIDE, 128), BF16),
        pltpu.VMEM((2, 2, 2, WIDE, 128), BF16),
        pltpu.VMEM((2, half, 128), BF16),
        pltpu.VMEM((2, 2, half, 128), BF16),
        pltpu.VMEM((2, half, 128), BF16),
        pltpu.VMEM((2, 2, half, 128), BF16),
        pltpu.VMEM((8, 2, ROWS, D), BF16),
        pltpu.VMEM((8, ROWS, D), BF16),
        pltpu.VMEM((2, 7, 64, D), BF16),
        pltpu.VMEM((4, 2, 8, WIDE), F32),
        pltpu.VMEM((4, 2, 8, WIDE), F32),
        pltpu.VMEM((2, 3, 8, 128), F32),
        pltpu.VMEM((8, 3, 8, 128), F32),
        pltpu.SemaphoreType.DMA((9,)),
        pltpu.SemaphoreType.DMA((N_COPIES,)),
        pltpu.SemaphoreType.DMA((N_COPIES,)),
    ]
    out = pl.pallas_call(
        kernel,
        out_shape=[
            jax.ShapeDtypeStruct((ROWS, D), BF16),
            jax.ShapeDtypeStruct((ROWS, WIDTH), F32),
            jax.ShapeDtypeStruct((ROWS, WIDTH), F32),
            jax.ShapeDtypeStruct((3, WIDTH), F32),
            jax.ShapeDtypeStruct((3, WIDTH), F32),
            jax.ShapeDtypeStruct((1, ROWS), F32),
            jax.ShapeDtypeStruct((1, ROWS), F32),
            jax.ShapeDtypeStruct((2, 3), F32),
        ],
        in_specs=[hbm, hbm, hbm, hbm, hbm, vmem, vmem, hbm],
        out_specs=[vmem] * 8,
        scratch_shapes=scratch,
        compiler_params=pltpu.CompilerParams(
            collective_id=0, has_side_effects=True, vmem_limit_bytes=67_000_000
        ),
        name="backward",
    )(tokens, up_gate, up_val, gate_weight, val_weight, gate_taps, val_taps, hidden_grad)
    return (*out[:5], out[5].reshape(ROWS), out[6].reshape(ROWS), out[7])


def solution(mesh):
    split = Mesh(mesh.devices.reshape(4, 4, 8, 2), ("y", "x", "z", "c"))
    fs, tp, both = ("y", "x"), ("z", "c"), ("y", "x", "z", "c")
    in_specs = (
        P(both, None), P(fs, tp), P(fs, tp), P(fs, tp), P(fs, tp), P(None, tp), P(None, tp), P(fs, tp),
    )
    out_specs = (
        P(both, None), P(fs, tp), P(fs, tp), P(None, tp), P(None, tp), P(fs), P(fs), P(),
    )
    return jax.shard_map(local, mesh=split, in_specs=in_specs, out_specs=out_specs, check_vma=False)
```

time: 235 us -> 120 us (0.51)
  Pallas kernels: 0 us -> 101 us
  other arithmetic: 68.9 us -> 0 us
  blocking collectives: 56.9 us -> 0 us
  matrix products: 33.7 us -> 0 us
  waiting for transfers between devices: 31.8 us -> 0 us
  between operations: 14 us -> 0.69 us
  starting transfers between devices: 10.7 us -> 0 us
    pallas_call x0 -> x1, Pallas kernels: none -> 101 us  [local(): pl.pallas_call(kernel, out_shape=[jax.ShapeDtypeStruct((ROWS, D), BF16),...]
    reduce_sum x9 -> x0, other arithmetic: 57.2 us -> none  [the longest x1 30.8 us: local_grads(): jnp.sum(padded_gate[:, tap_index:tap_index + length] * gate_back, axis=(0...]
    psum x2 -> x0, blocking collectives: 39 us -> none  [over_axes(): return functools.reduce(lax.psum, axes, value)]
    dot_general x4 -> x0, matrix products: 33.7 us -> none  [the longest x1 10.5 us: local(): lax.dot_general(val_back, val_whole, contract, preferred_element_type=jnp...]
    all_to_all x1 -> x0, blocking collectives: 17.9 us -> none  [from_everyone(): lax.all_to_all(jnp.broadcast_to(value[None], (size, *value.shape)), axis,...]
    all_gather x2 -> x0, waiting for transfers between devices: 16.6 us -> none  [the longest x1 16.6 us: local(): token_rows = lax.all_gather(tokens, 'tp', axis=0, tiled=True)]
    unnamed x16 -> x27, local copies, waits for them, and re-layouts: 0.79 us -> 17.2 us
    all_to_all x2 -> x0, waiting for transfers between devices: 14.4 us -> none  [sum_at_owner(): pieces = lax.all_to_all(cut_along(value, dim, size), axis, 0, 0, tiled=True)]
  transfers between devices with their start and end apart: 5 -> 0, of which waited for: 2 -> 0; matrix products, arithmetic and copies ran while one was open for 51% -> 0% of each run, Pallas kernels for 0% -> 0%
where the time goes in v1:
time: 120 us; the launch traced here: 119 us
  Pallas kernels  101 us (84%)
  local copies, waits for them, and re-layouts  17.2 us (14%)
    pallas_call x1, Pallas kernels, local(): pl.pallas_call(kernel, out_shape=[jax.ShapeDtypeStruct((ROWS, D), BF16),...  101 us
    unnamed x27, local copies, waits for them, and re-layouts  17.2 us

profile of v1, /device:TPU:1, one launch (start us, length us, event | category | flops | bytes accessed | tf_op | source)
XLA Modules:
  0.0 119.3 jit_solution(16292183875762837318)
XLA Ops:
  0.6 1.6 %copy.18.gw = bf16[128,352]{1,0:T(8,128)(2,1)} copy(bf16[128,352]{0,1:T(8,128)(2,1)} %param.11) | data formatting | bytes 180224 | tf_op args[3]
  2.3 0.0 copy-start
  2.3 1.7 %copy.19.vw = bf16[128,352]{1,0:T(8,128)(2,1)} copy(bf16[128,352]{0,1:T(8,128)(2,1)} %param.12) | data formatting | bytes 180224 | tf_op args[4]
  4.0 2.6 %copy.16.ug = bf16[2048,352]{1,0:T(8,128)(2,1)} copy(bf16[2048,352]{0,1:T(8,128)(2,1)} %param.9) | data formatting | bytes 2883584 | tf_op args[1]
  6.6 0.0 copy-done
  6.6 0.0 copy-start.1
  6.6 1.6 %copy.17.uv = bf16[2048,352]{1,0:T(8,128)(2,1)} copy(bf16[2048,352]{0,1:T(8,128)(2,1)S(1)} %copy-done) | data formatting | bytes 2883584 | tf_op args[2]
  8.2 0.0 copy-done.1
  8.2 1.6 %copy.20.hg = bf16[2048,352]{1,0:T(8,128)(2,1)} copy(bf16[2048,352]{0,1:T(8,128)(2,1)S(1)} %copy-done.1) | data formatting | bytes 2883584 | tf_op args[7]
  9.7 101.4 %backward.1 = (bf16[128,2048]{1,0:T(8,128)(2,1)}, f32[128,352]{1,0:T(8,128)}, f32[128,352]{1,0:T(8,128)}, f32[3,352]{1,0:T(4,128)}, f32[3,352]{1,0:T(4,128)}, /*...) custom-call(bf16[128,2048]{1,0:T(8,128)(2,1)} %tok.1, bf16[2048,352]{1,0:T(8,128)(2,1)} %copy.16.ug, ...), custom_call_target="tpu_custom_call" | custom-call | tf_op jit(solution)/shard_map/backward/pallas_call | solution.py:484
  111.1 0.0 copy-start.3
  111.1 0.0 copy-start.2
  111.1 0.0 copy-start.6
  111.2 0.0 copy-start.5
  111.2 0.0 copy-start.4
  111.2 1.7 %copy.21 = f32[128,352]{0,1:T(8,128)} copy(f32[128,352]{1,0:T(8,128)} %get-tuple-element.25) | data formatting | bytes 360448
  112.9 1.7 %copy.22 = f32[128,352]{0,1:T(8,128)} copy(f32[128,352]{1,0:T(8,128)} %get-tuple-element.26) | data formatting | bytes 360448
  114.6 1.9 %copy.29 = bf16[128,2048]{1,0:T(8,128)(2,1)} copy(bf16[128,2048]{1,0:T(8,128)(2,1)} %get-tuple-element.40) | data formatting | bytes 1048576
  116.5 0.0 copy-done.3
  116.5 0.6 copy.30
  117.1 0.0 copy-done.2
  117.1 0.6 copy.31
  117.7 0.0 copy-done.6
  117.7 0.5 copy.32
  118.2 0.0 copy-done.5
  118.2 0.5 copy.33
  118.7 0.0 copy-done.4
  118.7 0.6 copy.34
Async XLA Ops:
  2.3 4.3 %copy-start = (bf16[2048,352]{0,1:T(8,128)(2,1)S(1)}, bf16[2048,352]{0,1:T(8,128)(2,1)}, u32[]{:S(2)}) copy-start(bf16[2048,352]{0,1:T(8,128)(2,1)} %param.10) | copy-start | bytes 4325380
  6.6 1.6 %copy-start.1 = (bf16[2048,352]{0,1:T(8,128)(2,1)S(1)}, bf16[2048,352]{0,1:T(8,128)(2,1)}, u32[]{:S(2)}) copy-start(bf16[2048,352]{0,1:T(8,128)(2,1)} %param.15) | copy-start | bytes 4325380
  111.1 5.4 %copy-start.3 = (f32[3,352]{1,0:T(4,128)S(1)}, f32[3,352]{1,0:T(4,128)}, u32[]{:S(2)}) copy-start(f32[3,352]{1,0:T(4,128)} %get-tuple-element.43) | copy-start | bytes 12676
  111.1 6.0 %copy-start.2 = (f32[3,352]{1,0:T(4,128)S(1)}, f32[3,352]{1,0:T(4,128)}, u32[]{:S(2)}) copy-start(f32[3,352]{1,0:T(4,128)} %get-tuple-element.44) | copy-start | bytes 12676
  111.1 6.6 %copy-start.6 = (f32[1,128]{1,0:T(1,128)S(1)}, f32[1,128]{1,0:T(1,128)}, u32[]{:S(2)}) copy-start(f32[1,128]{1,0:T(1,128)} %get-tuple-element.21) | copy-start | bytes 1540
  111.2 7.1 %copy-start.5 = (f32[1,128]{1,0:T(1,128)S(1)}, f32[1,128]{1,0:T(1,128)}, u32[]{:S(2)}) copy-start(f32[1,128]{1,0:T(1,128)} %get-tuple-element.22) | copy-start | bytes 1540
  111.2 7.6 %copy-start.4 = (f32[2,3]{1,0:T(2,128)S(1)}, f32[2,3]{1,0:T(2,128)}, u32[]{:S(2)}) copy-start(f32[2,3]{1,0:T(2,128)} %get-tuple-element.47) | copy-start | bytes 76

commit v2 on v1

--- a/solution.py
+++ b/solution.py
@@ -14,10 +14,9 @@
 D = 2048
 ROWS = 128
 WIDTH = 352
-WIDE = 384
-PAD = 16
-CHUNK = 64
-NT = (((1,), (1,)), ((), ()))
+BOTH = 2 * WIDTH
+GROUP = 16
+TILES = SEQ // 128
 NN = (((1,), (0,)), ((), ()))
 N_COPIES = 106
 
@@ -25,7 +24,7 @@
 def kernel(
     tok, ug, uv, gw, vw, gt, vt, hg,
     ig_o, gwg_o, vwg_o, gtg_o, vtg_o, gn_o, vn_o, tn_o,
-    TOK, UGI, UVI, HGI, WT, UB, UBT, W, ACC, DA, DB, DA2, DB2,
+    TOK, UGI, UVI, HGI, KT, TS, UB, UBT, W, ACC, DA, DB, DA2, DB2,
     RA0, RA1, RB0, RB1, SA0, SA1, SB0, SB1, PB, PX, RS, TX, TY, NC, NZ,
     lsem, ssem, rsem,
 ):
@@ -55,18 +54,9 @@
 
     own_rows = pl.ds(pl.multiple_of(c * ROWS, ROWS), ROWS)
     l_tok = load(tok, TOK.at[z, own_rows], 0)
-    l_gw = load(gw, WT.at[0], 1)
-    l_vw = load(vw, WT.at[1], 2)
-    l_in = []
-    for s in range(2):
-        at = pl.ds(s * SEQ, SEQ)
-        l_in.append(
-            (
-                load(ug.at[at], UGI.at[s, pl.ds(PAD, SEQ)], 3 + 3 * s),
-                load(uv.at[at], UVI.at[s, pl.ds(PAD, SEQ)], 4 + 3 * s),
-                load(hg.at[at], HGI.at[s], 5 + 3 * s),
-            )
-        )
+    l_gw = load(gw, W.at[y, x, pl.ds(0, WIDTH)], 1)
+    l_vw = load(vw, W.at[y, x, pl.ds(WIDTH, WIDTH)], 2)
+    l_in = [load(a, b, 3 + i) for i, (a, b) in enumerate(((ug, UGI), (uv, UVI), (hg, HGI)))]
 
     barrier = pltpu.get_barrier_semaphore()
     peers = [{"c": p}]
@@ -76,11 +66,6 @@
     for peer in peers:
         pl.semaphore_signal(barrier, inc=1, device_id=peer, device_id_type=MESH)
 
-    l_gw.wait()
-    l_vw.wait()
-    W[y, x] = jnp.zeros((ROWS, 2 * WIDE), BF16)
-    W[y, x, :, 0:WIDTH] = WT[0]
-    W[y, x, :, WIDE : WIDE + WIDTH] = WT[1]
     l_tok.wait()
     pl.semaphore_wait(barrier, len(peers))
 
@@ -137,77 +122,91 @@
 
         return begin, middle, end
 
+    quarter = WIDTH // 2
+
     def a1(i, d):
-        return W.at[y, i, pl.ds(0, 64) if d is None else pl.ds(32 * d, 32)]
+        return W.at[y, i, pl.ds(0, WIDTH) if d is None else pl.ds(quarter * d, quarter)]
 
     def b1(i, d):
-        return W.at[i, x, pl.ds(64, 64) if d is None else pl.ds(64 + 32 * d, 32)]
+        rows = pl.ds(WIDTH, WIDTH) if d is None else pl.ds(WIDTH + quarter * d, quarter)
+        return W.at[i, x, rows]
 
     def a2(i, d):
-        return W.at[i, pl.ds(0, 4) if d is None else pl.ds(2 * d, 2), pl.ds(0, 64)]
+        return W.at[i, pl.ds(0, 4) if d is None else pl.ds(2 * d, 2), pl.ds(0, WIDTH)]
 
     def b2(i, d):
-        return W.at[pl.ds(0, 4) if d is None else pl.ds(2 * d, 2), i, pl.ds(64, 64)]
+        return W.at[pl.ds(0, 4) if d is None else pl.ds(2 * d, 2), i, pl.ds(WIDTH, WIDTH)]
 
     first = gather(a1, "x", x), gather(b1, "y", y)
     second = gather(a2, "y", y), gather(b2, "x", x)
+    l_gw.wait()
+    l_vw.wait()
     for g in first:
         g[0]()
 
-    for s in range(2):
-        UGI[s, 0:PAD] = jnp.zeros((PAD, WIDTH), BF16)
-        UVI[s, 0:PAD] = jnp.zeros((PAD, WIDTH), BF16)
-    UB[:, 256:384] = jnp.zeros((2 * SEQ, 128), BF16)
-    UB[:, 640:768] = jnp.zeros((2 * SEQ, 128), BF16)
-    TX[x] = jnp.zeros((2, 8, WIDE), F32)
-
-    def conv(s, t):
-        lo, hi = t * 128, min(t * 128 + 128, WIDTH)
-        n = hi - lo
-        kg = [gt[i : i + 1, lo:hi].astype(F32) for i in range(3)]
-        kv = [vt[i : i + 1, lo:hi].astype(F32) for i in range(3)]
-
-        def fold(a):
-            return jnp.sum(a.reshape(CHUNK // 8, 8, n), axis=0)
-
-        def step(j, carry):
-            sums, gb_next, vb_next = carry
-            r = pl.multiple_of((SEQ // CHUNK - 1 - j) * CHUNK, CHUNK)
-            g = UGI[s, pl.ds(r, CHUNK + PAD), lo:hi].astype(F32)
-            v = UVI[s, pl.ds(r, CHUNK + PAD), lo:hi].astype(F32)
-            h = HGI[s, pl.ds(r, CHUNK), lo:hi].astype(F32)
-            gs = [g[PAD - 2 + i : PAD - 2 + i + CHUNK] for i in range(3)]
-            vs = [v[PAD - 2 + i : PAD - 2 + i + CHUNK] for i in range(3)]
-            cg = kg[0] * gs[0] + kg[1] * gs[1] + kg[2] * gs[2]
-            cv = kv[0] * vs[0] + kv[1] * vs[1] + kv[2] * vs[2]
-            sg = jax.nn.sigmoid(cg)
-            hs = h * sg
-            vb = hs * cg
-            gb = hs * cv * (1.0 + cg * (1.0 - sg))
-            sums = tuple(
-                a + fold(b)
-                for a, b in zip(sums, [u * gb for u in gs] + [u * vb for u in vs])
-            )
-            gx = jnp.concatenate([gb, gb_next], axis=0)
-            vx = jnp.concatenate([vb, vb_next], axis=0)
-            og = kg[2] * gb + kg[1] * gx[1 : CHUNK + 1] + kg[0] * gx[2 : CHUNK + 2]
-            ov = kv[2] * vb + kv[1] * vx[1 : CHUNK + 1] + kv[0] * vx[2 : CHUNK + 2]
-            at = pl.ds(s * SEQ + r, CHUNK)
-            UB[at, lo:hi] = og.astype(BF16)
-            UB[at, WIDE + lo : WIDE + hi] = ov.astype(BF16)
-            return sums, gb[0:8], vb[0:8]
-
-        zero = jnp.zeros((8, n), F32)
-        sums, _, _ = lax.fori_loop(0, SEQ // CHUNK, step, ((zero,) * 6, zero, zero))
-        for i in range(3):
+    for q, ref in enumerate((gt, vt)):
+        rows = jnp.concatenate([ref[...].astype(F32), jnp.zeros((5, WIDTH), F32)], axis=0)
+        for t in range(3):
+            lo, hi = t * 128, min(t * 128 + 128, WIDTH)
+            KT[q, lo:hi, 0:8] = rows[:, lo:hi].T
+
+    lane = lax.broadcasted_iota(jnp.int32, (GROUP, 128), 1)
+    edge = {1: lane >= 1, 2: lane >= 2, -1: lane < 127, -2: lane < 126}
+    nil = jnp.zeros((GROUP, 128), F32)
+
+    def moved(tiles, k):
+        turned = [pltpu.roll(a, k % 128, 1) for a in tiles]
+        if k > 0:
+            other = [nil] + turned[:-1]
+        else:
+            other = turned[1:] + [nil]
+        return [jnp.where(edge[k], a, b) for a, b in zip(turned, other)]
+
+    def conv(first_group, last_group):
+        def step(g, _):
+            rows = pl.ds(pl.multiple_of(g * GROUP, GROUP), GROUP)
+            low = pl.ds(pl.multiple_of(WIDTH + g * GROUP, GROUP), GROUP)
+            kg = [jnp.broadcast_to(KT[0, rows, i : i + 1], (GROUP, 128)) for i in range(3)]
+            kv = [jnp.broadcast_to(KT[1, rows, i : i + 1], (GROUP, 128)) for i in range(3)]
+            sums = [nil] * 6
+            for s in range(2):
+                at = [slice(s * SEQ + i * 128, s * SEQ + i * 128 + 128) for i in range(TILES)]
+                g0 = [UGI[rows, a].astype(F32) for a in at]
+                v0 = [UVI[rows, a].astype(F32) for a in at]
+                g1, g2, v1, v2 = moved(g0, 1), moved(g0, 2), moved(v0, 1), moved(v0, 2)
+                gb, vb = [], []
+                for i in range(TILES):
+                    h = HGI[rows, at[i]].astype(F32)
+                    cg = kg[0] * g2[i] + kg[1] * g1[i] + kg[2] * g0[i]
+                    cv = kv[0] * v2[i] + kv[1] * v1[i] + kv[2] * v0[i]
+                    sg = jax.nn.sigmoid(cg)
+                    hs = h * sg
+                    vb.append(hs * cg)
+                    gb.append(hs * cv * (1.0 + cg * (1.0 - sg)))
+                    terms = [u * gb[i] for u in (g2[i], g1[i], g0[i])]
+                    terms += [u * vb[i] for u in (v2[i], v1[i], v0[i])]
+                    sums = [a + b for a, b in zip(sums, terms)]
+                gb1, gb2, vb1, vb2 = moved(gb, -1), moved(gb, -2), moved(vb, -1), moved(vb, -2)
+                for i in range(TILES):
+                    half = slice((i % 2) * 128, (i % 2) * 128 + 128)
+                    og = kg[2] * gb[i] + kg[1] * gb1[i] + kg[0] * gb2[i]
+                    ov = kv[2] * vb[i] + kv[1] * vb1[i] + kv[0] * vb2[i]
+                    UBT[4 * s + i // 2, rows, half] = og.astype(BF16)
+                    UBT[4 * s + i // 2, low, half] = ov.astype(BF16)
             for q in range(2):
-                TX[x, q, i : i + 1, lo:hi] += jnp.sum(sums[3 * q + i], axis=0, keepdims=True)
+                t = [jnp.sum(sums[3 * q + i], axis=1, keepdims=True) for i in range(3)]
+                TS[q, rows, :] = jnp.where(
+                    lane == 0, t[0], jnp.where(lane == 1, t[1], jnp.where(lane == 2, t[2], 0.0))
+                )
+            return 0
+
+        lax.fori_loop(first_group, last_group, step, 0)
 
     def turn(zz):
-        for t in range(6):
-            UBT[zz, t * 128 : t * 128 + 128, :] = UB[
-                pl.ds(pl.multiple_of(zz * 256, 256), 256), t * 128 : t * 128 + 128
-            ].T
+        rows = pl.ds(pl.multiple_of(zz * 256, 256), 256)
+        for lo in range(0, BOTH, 128):
+            hi = min(lo + 128, BOTH)
+            UB[rows, lo:hi] = UBT[zz, lo:hi, :].T
 
     def weight_part(ks, first_part=False, last_part=False):
         zs = [ahead(z, k, 8) for k in ks]
@@ -224,8 +223,8 @@
                 out = total.astype(BF16)
                 yy, xx = n // 2, 2 * (n % 2)
                 for q in range(2):
-                    DA[xx + q, yy // 2, yy % 2] = out[0:WIDE, q * 128 : q * 128 + 128]
-                    DB[yy, xx // 2, q] = out[WIDE : 2 * WIDE, q * 128 : q * 128 + 128]
+                    DA[xx + q, yy // 2, yy % 2] = out[0:WIDTH, q * 128 : q * 128 + 128]
+                    DB[yy, xx // 2, q] = out[WIDTH:BOTH, q * 128 : q * 128 + 128]
             else:
                 ACC[n] = total
             return 0
@@ -244,8 +243,9 @@
         rows = pl.ds(pl.multiple_of(zz * 256, 256), 256)
 
         def step(n, _):
-            w = W[n // 2, pl.ds(2 * (n % 2), 2)].reshape(256, 2 * WIDE)
-            out = lax.dot_general(UB[rows, :], w, NT, preferred_element_type=F32).astype(BF16)
+            yy, xx = n // 2, 2 * (n % 2)
+            w = jnp.concatenate([W[yy, xx], W[yy, xx + 1]], axis=1)
+            out = lax.dot_general(UB[rows, :], w, NN, preferred_element_type=F32).astype(BF16)
             cols = pl.ds(pl.multiple_of(n * 256, 256), 256)
             PB[k, 0, :, cols] = out[0:128]
             PB[k, 1, :, cols] = out[128:256]
@@ -319,19 +319,21 @@
     def tap_sum(ref):
         return ref[0] + ref[1] + ref[2] + ref[3]
 
-    for s in range(2):
-        for copy in l_in[s]:
-            copy.wait()
-        for t in range(3):
-            conv(s, t)
-            if s == 0 and t == 1:
-                for g in first:
-                    g[1]()
-            if s == 1 and t == 0:
-                for g in first:
-                    g[2]()
-                for g in second:
-                    g[0]()
+    for copy in l_in:
+        copy.wait()
+    conv(0, 8)
+    for g in first:
+        g[1]()
+    conv(8, 16)
+    for g in first:
+        g[2]()
+    for g in second:
+        g[0]()
+    conv(16, 22)
+    for q in range(2):
+        for lo in range(0, WIDTH, 128):
+            hi = min(lo + 128, WIDTH)
+            TX[x, q, :, lo:hi] = TS[q, lo:hi, :].T[0:8]
     tap_x = [remote(TX.at[x], TX.at[x], x=ahead(x, k, 4)) for k in (1, 2, 3)]
     tok_event(0)
     lax.fori_loop(0, 8, lambda i, _: (turn(i), 0)[1], 0)
@@ -386,8 +388,8 @@
     sc_a1[2]()
     sc_b1[2]()
     for q in range(4):
-        DA2[q] = sc_a1[3](q // 2, q % 2).astype(BF16).reshape(2, 192, 128)
-        DB2[q] = sc_b1[3](q // 2, q % 2).astype(BF16).reshape(2, 192, 128)
+        DA2[q] = sc_a1[3](q // 2, q % 2).astype(BF16).reshape(2, quarter, 128)
+        DB2[q] = sc_b1[3](q // 2, q % 2).astype(BF16).reshape(2, quarter, 128)
     sc_a2[0]()
     sc_b2[0]()
     sum_event(5)
@@ -398,9 +400,9 @@
     sc_b2[2]()
     norms = []
     for scat, out in ((sc_a2, gwg_o), (sc_b2, vwg_o)):
-        grad = scat[3]().reshape(WIDE, 128)
+        grad = scat[3]().reshape(WIDTH, 128)
         norms.append(jnp.sum(grad * grad, axis=0, keepdims=True))
-        out[...] = grad.T[:, 0:WIDTH]
+        out[...] = grad
     NC[c, 0, 0:1] = norms[0]
     NC[c, 0, 1:2] = norms[1]
     pair = remote(NC.at[c], NC.at[c], c=p)
@@ -444,28 +446,34 @@
     assert len(started) == N_COPIES, len(started)
 
 
+def finish(*refs):
+    for src, dst in zip(refs[:8], refs[8:]):
+        dst[...] = src[...]
+
+
 def local(tokens, up_gate, up_val, gate_weight, val_weight, gate_taps, val_taps, hidden_grad):
     hbm = pl.BlockSpec(memory_space=pl.ANY)
     vmem = pl.BlockSpec(memory_space=pltpu.VMEM)
-    half = WIDE // 2
+    half = WIDTH // 2
     scratch = [
         pltpu.VMEM((8, 256, D), BF16),
-        pltpu.VMEM((2, PAD + SEQ, WIDTH), BF16),
-        pltpu.VMEM((2, PAD + SEQ, WIDTH), BF16),
-        pltpu.VMEM((2, SEQ, WIDTH), BF16),
-        pltpu.VMEM((2, ROWS, WIDTH), BF16),
-        pltpu.VMEM((2 * SEQ, 2 * WIDE), BF16),
-        pltpu.VMEM((8, 2 * WIDE, 256), BF16),
-        pltpu.VMEM((4, 4, ROWS, 2 * WIDE), BF16),
-        pltpu.VMEM((8, 2 * WIDE, 256), F32),
-        pltpu.VMEM((4, 2, 2, WIDE, 128), BF16),
-        pltpu.VMEM((4, 2, 2, WIDE, 128), BF16),
+        pltpu.VMEM((WIDTH, 2 * SEQ), BF16),
+        pltpu.VMEM((WIDTH, 2 * SEQ), BF16),
+        pltpu.VMEM((WIDTH, 2 * SEQ), BF16),
+        pltpu.VMEM((2, WIDTH, 128), F32),
+        pltpu.VMEM((2, WIDTH, 128), F32),
+        pltpu.VMEM((2 * SEQ, BOTH), BF16),
+        pltpu.VMEM((8, BOTH, 256), BF16),
+        pltpu.VMEM((4, 4, BOTH, ROWS), BF16),
+        pltpu.VMEM((8, BOTH, 256), F32),
+        pltpu.VMEM((4, 2, 2, WIDTH, 128), BF16),
+        pltpu.VMEM((4, 2, 2, WIDTH, 128), BF16),
         pltpu.VMEM((4, 2, half, 128), BF16),
         pltpu.VMEM((4, 2, half, 128), BF16),
-        pltpu.VMEM((2, 2, WIDE, 128), BF16),
-        pltpu.VMEM((2, 2, 2, WIDE, 128), BF16),
-        pltpu.VMEM((2, 2, WIDE, 128), BF16),
-        pltpu.VMEM((2, 2, 2, WIDE, 128), BF16),
+        pltpu.VMEM((2, 2, WIDTH, 128), BF16),
+        pltpu.VMEM((2, 2, 2, WIDTH, 128), BF16),
+        pltpu.VMEM((2, 2, WIDTH, 128), BF16),
+        pltpu.VMEM((2, 2, 2, WIDTH, 128), BF16),
         pltpu.VMEM((2, half, 128), BF16),
         pltpu.VMEM((2, 2, half, 128), BF16),
         pltpu.VMEM((2, half, 128), BF16),
@@ -473,11 +481,11 @@
         pltpu.VMEM((8, 2, ROWS, D), BF16),
         pltpu.VMEM((8, ROWS, D), BF16),
         pltpu.VMEM((2, 7, 64, D), BF16),
-        pltpu.VMEM((4, 2, 8, WIDE), F32),
-        pltpu.VMEM((4, 2, 8, WIDE), F32),
+        pltpu.VMEM((4, 2, 8, WIDTH), F32),
+        pltpu.VMEM((4, 2, 8, WIDTH), F32),
         pltpu.VMEM((2, 3, 8, 128), F32),
         pltpu.VMEM((8, 3, 8, 128), F32),
-        pltpu.SemaphoreType.DMA((9,)),
+        pltpu.SemaphoreType.DMA((6,)),
         pltpu.SemaphoreType.DMA((N_COPIES,)),
         pltpu.SemaphoreType.DMA((N_COPIES,)),
     ]
@@ -485,8 +493,8 @@
         kernel,
         out_shape=[
             jax.ShapeDtypeStruct((ROWS, D), BF16),
-            jax.ShapeDtypeStruct((ROWS, WIDTH), F32),
-            jax.ShapeDtypeStruct((ROWS, WIDTH), F32),
+            jax.ShapeDtypeStruct((WIDTH, ROWS), F32),
+            jax.ShapeDtypeStruct((WIDTH, ROWS), F32),
             jax.ShapeDtypeStruct((3, WIDTH), F32),
             jax.ShapeDtypeStruct((3, WIDTH), F32),
             jax.ShapeDtypeStruct((1, ROWS), F32),
@@ -500,8 +508,15 @@
             collective_id=0, has_side_effects=True, vmem_limit_bytes=67_000_000
         ),
         name="backward",
-    )(tokens, up_gate, up_val, gate_weight, val_weight, gate_taps, val_taps, hidden_grad)
-    return (*out[:5], out[5].reshape(ROWS), out[6].reshape(ROWS), out[7])
+    )(tokens, up_gate.T, up_val.T, gate_weight.T, val_weight.T, gate_taps, val_taps, hidden_grad.T)
+    out = pl.pallas_call(
+        finish,
+        out_shape=[jax.ShapeDtypeStruct(a.shape, a.dtype) for a in out],
+        in_specs=[vmem] * 8,
+        out_specs=[vmem] * 8,
+        name="finish",
+    )(*out)
+    return (out[0], out[1].T, out[2].T, out[3], out[4], out[5].reshape(ROWS), out[6].reshape(ROWS), out[7])
 
 
 def solution(mesh):

time: 120 us -> 102 us (0.85)
  local copies, waits for them, and re-layouts: 17.2 us -> 0 us
    unnamed x27 -> x0, local copies, waits for them, and re-layouts: 17.2 us -> none
    pallas_call x1, Pallas kernels: 101 us -> 98.4 us  [local(): pl.pallas_call(kernel, out_shape=[jax.ShapeDtypeStruct((ROWS, D), BF16),...]
    pallas_call x0 -> x1, Pallas kernels: none -> 2.14 us  [local(): pl.pallas_call(finish, out_shape=[jax.ShapeDtypeStruct(a.shape, a.dtype)...]
where the time goes in v2:
time: 102 us; the launch traced here: 101 us
  Pallas kernels  101 us (99%)
    pallas_call x1, Pallas kernels, local(): pl.pallas_call(kernel, out_shape=[jax.ShapeDtypeStruct((ROWS, D), BF16),...  98.4 us
    pallas_call x1, Pallas kernels, local(): pl.pallas_call(finish, out_shape=[jax.ShapeDtypeStruct(a.shape, a.dtype)...  2.14 us

profile of v2, /device:TPU:1, one launch (start us, length us, event | category | flops | bytes accessed | tf_op | source)
XLA Modules:
  0.0 101.2 jit_solution(3262560910862495031)
XLA Ops:
  0.6 98.4 %backward.1 = (bf16[128,2048]{1,0:T(8,128)(2,1)}, f32[352,128]{1,0:T(8,128)}, f32[352,128]{1,0:T(8,128)}, f32[3,352]{1,0:T(4,128)}, f32[3,352]{1,0:T(4,128)}, /*...) custom-call(bf16[128,2048]{1,0:T(8,128)(2,1)} %tok.1, bf16[352,2048]{1,0:T(8,128)(2,1)} %bitcast.9, ...), custom_call_target="tpu_custom_call" | custom-call | tf_op jit(solution)/shard_map/backward/pallas_call | solution.py:492
  99.1 2.1 %finish.1 = (bf16[128,2048]{1,0:T(8,128)(2,1)}, f32[352,128]{1,0:T(8,128)}, f32[352,128]{1,0:T(8,128)}, f32[3,352]{1,0:T(4,128)}, f32[3,352]{1,0:T(4,128)}, /*in...) custom-call(bf16[128,2048]{1,0:T(8,128)(2,1)} %get-tuple-element.24.refs_0_, ...), custom_call_target="tpu_custom_call" | custom-call | tf_op jit(solution)/shard_map/finish/pallas_call | solution.py:512

commit v3 on v2

--- a/solution.py
+++ b/solution.py
@@ -23,8 +23,8 @@
 
 def kernel(
     tok, ug, uv, gw, vw, gt, vt, hg,
-    ig_o, gwg_o, vwg_o, gtg_o, vtg_o, gn_o, vn_o, tn_o,
-    TOK, UGI, UVI, HGI, KT, TS, UB, UBT, W, ACC, DA, DB, DA2, DB2,
+    own_o, cross_o, last_o, gwg_o, vwg_o, small_o,
+    TOK, UGI, UVI, HGI, GT, VT, SM, GW, KT, TS, UB, UBT, W, ACC, DA, DB, DA2, DB2,
     RA0, RA1, RB0, RB1, SA0, SA1, SB0, SB1, PB, PX, RS, TX, TY, NC, NZ,
     lsem, ssem, rsem,
 ):
@@ -56,7 +56,8 @@
     l_tok = load(tok, TOK.at[z, own_rows], 0)
     l_gw = load(gw, W.at[y, x, pl.ds(0, WIDTH)], 1)
     l_vw = load(vw, W.at[y, x, pl.ds(WIDTH, WIDTH)], 2)
-    l_in = [load(a, b, 3 + i) for i, (a, b) in enumerate(((ug, UGI), (uv, UVI), (hg, HGI)))]
+    pairs = (gt, GT), (vt, VT), (ug, UGI), (uv, UVI), (hg, HGI)
+    l_in = [load(a, b, 3 + i) for i, (a, b) in enumerate(pairs)]
 
     barrier = pltpu.get_barrier_semaphore()
     peers = [{"c": p}]
@@ -144,7 +145,9 @@
     for g in first:
         g[0]()
 
-    for q, ref in enumerate((gt, vt)):
+    for copy in l_in:
+        copy.wait()
+    for q, ref in enumerate((GT, VT)):
         rows = jnp.concatenate([ref[...].astype(F32), jnp.zeros((5, WIDTH), F32)], axis=0)
         for t in range(3):
             lo, hi = t * 128, min(t * 128 + 128, WIDTH)
@@ -252,7 +255,7 @@
             return 0
 
         lax.fori_loop(0, 8, step, 0)
-        partner[k] = remote(PB.at[k, p], PX.at[k], c=p)
+        partner[k] = remote(PB.at[k, p], PX.at[k] if k else cross_o, c=p)
 
     sum_up = [(0, 0), (1, 1), (1, 0), (2, 1), (2, 0), (3, 1), (3, 0)]
     flow = {}
@@ -280,7 +283,9 @@
                 flow[d, j - 2].wait_recv()
             pair_sum(k, h, (d, j - 2) if j >= 2 else None)
             flow[d, j] = remote(
-                PB.at[k, c, pl.ds(h * 64, 64)], RS.at[d, j], z=ahead(z, 1 if d == 0 else 7, 8)
+                PB.at[k, c, pl.ds(h * 64, 64)],
+                RS.at[d, j] if s < 3 else last_o.at[d, pl.ds(h * 64, 64)],
+                z=ahead(z, 1 if d == 0 else 7, 8),
             )
 
     def scatter(src, r0, r1, axis, i):
@@ -319,72 +324,71 @@
     def tap_sum(ref):
         return ref[0] + ref[1] + ref[2] + ref[3]
 
-    for copy in l_in:
-        copy.wait()
     conv(0, 8)
     for g in first:
         g[1]()
-    conv(8, 16)
+    conv(8, 15)
+    tok_event(0)
     for g in first:
         g[2]()
     for g in second:
         g[0]()
-    conv(16, 22)
+    conv(15, 22)
     for q in range(2):
         for lo in range(0, WIDTH, 128):
             hi = min(lo + 128, WIDTH)
             TX[x, q, :, lo:hi] = TS[q, lo:hi, :].T[0:8]
     tap_x = [remote(TX.at[x], TX.at[x], x=ahead(x, k, 4)) for k in (1, 2, 3)]
-    tok_event(0)
     lax.fori_loop(0, 8, lambda i, _: (turn(i), 0)[1], 0)
     tok_event(1)
+    wait_cross(0)
+    weight_part([0], first_part=True)
+    wait_cross(1, 7)
+    weight_part([1, 7])
+    for g in second:
+        g[1]()
+    tok_event(2)
     for copy in tap_x:
         copy.wait_recv()
     TY[y] = tap_sum(TX)
     tap_y = [remote(TY.at[y], TY.at[y], y=ahead(y, k, 4)) for k in (1, 2, 3)]
-    wait_cross(0)
-    weight_part([0], first_part=True)
-    tok_event(2)
-    for g in second:
-        g[1]()
-    wait_cross(1, 7)
-    weight_part([1, 7])
     tok_event(3)
-    for copy in tap_y:
-        copy.wait_recv()
-    taps = tap_sum(TY)
-    gtg_o[...] = taps[0, 0:3, 0:WIDTH]
-    vtg_o[...] = taps[1, 0:3, 0:WIDTH]
-    NC[c, 1] = jnp.broadcast_to(jnp.sum(taps[0] * taps[0], axis=1, keepdims=True), (8, 128))
-    NC[c, 2] = jnp.broadcast_to(jnp.sum(taps[1] * taps[1], axis=1, keepdims=True), (8, 128))
-    tok_event(4)
     for g in second:
         g[2]()
     input_part(4)
     input_part(3)
+    tok_event(4)
     input_part(5)
-    tok_event(5)
     sum_event(0)
     sum_event(1)
     wait_cross(2, 6)
     weight_part([2, 6])
-    tok_event(6)
+    tok_event(5)
+    input_part(2)
     wait_cross(3, 5)
     weight_part([3, 5])
+    tok_event(6)
     wait_cross(4)
     weight_part([4], last_part=True)
     sc_a1[0]()
     sc_b1[0]()
-    input_part(2)
     input_part(6)
     sum_event(2)
     input_part(1)
-    sum_event(3)
+    input_part(7)
     sc_a1[1]()
     sc_b1[1]()
-    input_part(7)
+    sum_event(3)
+    input_part(0)
+    own = load(PB.at[0, c], own_o, 0)
+    for copy in tap_y:
+        copy.wait_recv()
+    taps = tap_sum(TY)
+    for q in range(2):
+        SM[8 * q : 8 * q + 8, :] = taps[q]
+        square = jnp.sum(taps[q] * taps[q], axis=1, keepdims=True)
+        NC[c, 1 + q] = jnp.broadcast_to(square, (8, 128))
     sum_event(4)
-    input_part(0)
     sc_a1[2]()
     sc_b1[2]()
     for q in range(4):
@@ -392,63 +396,56 @@
         DB2[q] = sc_b1[3](q // 2, q % 2).astype(BF16).reshape(2, quarter, 128)
     sc_a2[0]()
     sc_b2[0]()
-    sum_event(5)
     sc_a2[1]()
     sc_b2[1]()
-    sum_event(6)
+    sum_event(5)
     sc_a2[2]()
     sc_b2[2]()
-    norms = []
-    for scat, out in ((sc_a2, gwg_o), (sc_b2, vwg_o)):
+    NC[c, 0] = jnp.zeros((8, 128), F32)
+    for q, scat in enumerate((sc_a2, sc_b2)):
         grad = scat[3]().reshape(WIDTH, 128)
-        norms.append(jnp.sum(grad * grad, axis=0, keepdims=True))
-        out[...] = grad
-    NC[c, 0, 0:1] = norms[0]
-    NC[c, 0, 1:2] = norms[1]
+        NC[c, 0, q : q + 1] = jnp.sum(grad * grad, axis=0, keepdims=True)
+        GW[q] = grad
     pair = remote(NC.at[c], NC.at[c], c=p)
+    results = [load(GW.at[0], gwg_o, 1), load(GW.at[1], vwg_o, 2)]
     pair.wait_recv()
     NZ[z] = NC[0] + NC[1]
     along = [remote(NZ.at[z], NZ.at[z], z=ahead(z, k, 8)) for k in range(1, 8)]
-    partner[0].wait_recv()
-    for d in range(2):
-        flow[d, 5].wait_recv()
-        flow[d, 6].wait_recv()
-
-    for h in range(2):
-        j_up = 6 if h == 0 else 5
-        j_dn = 5 if h == 0 else 6
-
-        def step(i, _, h=h, j_up=j_up, j_dn=j_dn):
-            rows = pl.ds(pl.multiple_of(h * 64 + i * 16, 16), 16)
-            here = pl.ds(pl.multiple_of(i * 16, 16), 16)
-            v = PB[0, c, rows, :].astype(F32) + PX[0, rows, :].astype(F32)
-            v = v + RS[0, j_up, here, :].astype(F32) + RS[1, j_dn, here, :].astype(F32)
-            ig_o[rows, :] = v.astype(BF16)
-            return 0
-
-        lax.fori_loop(0, 4, step, 0)
-
+    sum_event(6)
     for copy in along:
         copy.wait_recv()
     total = NZ[0]
     for k in range(1, 8):
         total = total + NZ[k]
-    gn_o[...] = total[0, 0:1]
-    vn_o[...] = total[0, 1:2]
     diagonal = lax.broadcasted_iota(jnp.int32, (8, 128), 0) == lax.broadcasted_iota(
         jnp.int32, (8, 128), 1
     )
+    SM[16:24, 0:128] = total[0]
     for q in range(2):
         row = jnp.sum(jnp.where(diagonal, total[1 + q], 0.0), axis=0, keepdims=True)
-        tn_o[q : q + 1, :] = row[:, 0:3]
+        SM[18 + q : 19 + q, 0:128] = row
+    small = load(SM, small_o, 3)
+    for copy in (own, *results, small):
+        copy.wait()
+    partner[0].wait_recv()
+    for d in range(2):
+        flow[d, 5].wait_recv()
+        flow[d, 6].wait_recv()
     for copy in started:
         copy.wait_send()
     assert len(started) == N_COPIES, len(started)
 
 
-def finish(*refs):
-    for src, dst in zip(refs[:8], refs[8:]):
-        dst[...] = src[...]
+def finish(own, cross, last, gwg, vwg, small, ig_o, gwg_o, vwg_o, gtg_o, vtg_o, gn_o, vn_o, tn_o):
+    gwg_o[...] = gwg[...]
+    vwg_o[...] = vwg[...]
+    gtg_o[...] = small[0:3, :]
+    vtg_o[...] = small[8:11, :]
+    gn_o[...] = small[16:17, 0:128]
+    vn_o[...] = small[17:18, 0:128]
+    tn_o[...] = small[18:20, 0:3]
+    value = own[...].astype(F32) + cross[...].astype(F32)
+    ig_o[...] = (value + last[0].astype(F32) + last[1].astype(F32)).astype(BF16)
 
 
 def local(tokens, up_gate, up_val, gate_weight, val_weight, gate_taps, val_taps, hidden_grad):
@@ -460,6 +457,10 @@
         pltpu.VMEM((WIDTH, 2 * SEQ), BF16),
         pltpu.VMEM((WIDTH, 2 * SEQ), BF16),
         pltpu.VMEM((WIDTH, 2 * SEQ), BF16),
+        pltpu.VMEM((3, WIDTH), BF16),
+        pltpu.VMEM((3, WIDTH), BF16),
+        pltpu.VMEM((24, WIDTH), F32),
+        pltpu.VMEM((2, WIDTH, ROWS), F32),
         pltpu.VMEM((2, WIDTH, 128), F32),
         pltpu.VMEM((2, WIDTH, 128), F32),
         pltpu.VMEM((2 * SEQ, BOTH), BF16),
@@ -485,12 +486,30 @@
         pltpu.VMEM((4, 2, 8, WIDTH), F32),
         pltpu.VMEM((2, 3, 8, 128), F32),
         pltpu.VMEM((8, 3, 8, 128), F32),
-        pltpu.SemaphoreType.DMA((6,)),
+        pltpu.SemaphoreType.DMA((8,)),
         pltpu.SemaphoreType.DMA((N_COPIES,)),
         pltpu.SemaphoreType.DMA((N_COPIES,)),
     ]
     out = pl.pallas_call(
         kernel,
+        out_shape=[
+            jax.ShapeDtypeStruct((ROWS, D), BF16),
+            jax.ShapeDtypeStruct((ROWS, D), BF16),
+            jax.ShapeDtypeStruct((2, ROWS, D), BF16),
+            jax.ShapeDtypeStruct((WIDTH, ROWS), F32),
+            jax.ShapeDtypeStruct((WIDTH, ROWS), F32),
+            jax.ShapeDtypeStruct((24, WIDTH), F32),
+        ],
+        in_specs=[hbm] * 8,
+        out_specs=[hbm] * 6,
+        scratch_shapes=scratch,
+        compiler_params=pltpu.CompilerParams(
+            collective_id=0, has_side_effects=True, vmem_limit_bytes=67_000_000
+        ),
+        name="backward",
+    )(tokens, up_gate.T, up_val.T, gate_weight.T, val_weight.T, gate_taps, val_taps, hidden_grad.T)
+    out = pl.pallas_call(
+        finish,
         out_shape=[
             jax.ShapeDtypeStruct((ROWS, D), BF16),
             jax.ShapeDtypeStruct((WIDTH, ROWS), F32),
@@ -501,18 +520,7 @@
             jax.ShapeDtypeStruct((1, ROWS), F32),
             jax.ShapeDtypeStruct((2, 3), F32),
         ],
-        in_specs=[hbm, hbm, hbm, hbm, hbm, vmem, vmem, hbm],
-        out_specs=[vmem] * 8,
-        scratch_shapes=scratch,
-        compiler_params=pltpu.CompilerParams(
-            collective_id=0, has_side_effects=True, vmem_limit_bytes=67_000_000
-        ),
-        name="backward",
-    )(tokens, up_gate.T, up_val.T, gate_weight.T, val_weight.T, gate_taps, val_taps, hidden_grad.T)
-    out = pl.pallas_call(
-        finish,
-        out_shape=[jax.ShapeDtypeStruct(a.shape, a.dtype) for a in out],
-        in_specs=[vmem] * 8,
+        in_specs=[vmem] * 6,
         out_specs=[vmem] * 8,
         name="finish",
     )(*out)

time: 102 us -> 96.4 us (0.945)
  Pallas kernels: 101 us -> 95.6 us
    pallas_call x1, Pallas kernels: 98.4 us -> 92.9 us  [local(): pl.pallas_call(kernel, out_shape=[jax.ShapeDtypeStruct((ROWS, D), BF16),...]
where the time goes in v3:
time: 96.4 us; the launch traced here: 96.3 us
  Pallas kernels  95.6 us (99%)
    pallas_call x1, Pallas kernels, local(): pl.pallas_call(kernel, out_shape=[jax.ShapeDtypeStruct((ROWS, D), BF16),...  92.9 us
    pallas_call x1, Pallas kernels, local(): pl.pallas_call(finish, out_shape=[jax.ShapeDtypeStruct((ROWS, D), BF16),...  2.7 us

profile of v3, /device:TPU:1, one launch (start us, length us, event | category | flops | bytes accessed | tf_op | source)
XLA Modules:
  0.0 96.3 jit_solution(606875382456916690)
XLA Ops:
  0.6 92.9 %backward.1 = (bf16[128,2048]{1,0:T(8,128)(2,1)}, bf16[128,2048]{1,0:T(8,128)(2,1)}, bf16[2,128,2048]{2,1,0:T(8,128)(2,1)}, f32[352,128]{1,0:T(8,128)}, f32[352,128]{1,0:T(8,128)}, /*index=5*/f32[24,352]{1,0:T(8,128)}) custom-call(bf16[128,2048]{1,0:T(8,128)(2,1)} %tok.1, bf16[352,2048]{1,0:T(8,128)(2,1)} %bitcast.9, bf16[352,2048]{1,0:T(8,128)(2,1)} %bitcast.10, ...), custom_call_target="tpu_custom_call" | custom-call | tf_op jit(solution)/shard_map/backward/pallas_call | solution.py:493
  93.6 2.7 %finish.1 = (bf16[128,2048]{1,0:T(8,128)(2,1)}, f32[352,128]{1,0:T(8,128)}, f32[352,128]{1,0:T(8,128)}, f32[3,352]{1,0:T(4,128)}, f32[3,352]{1,0:T(4,128)}, /*in...) custom-call(bf16[128,2048]{1,0:T(8,128)(2,1)} %get-tuple-element.22.own, ...), custom_call_target="tpu_custom_call" | custom-call | tf_op jit(solution)/shard_map/finish/pallas_call | solution.py:511

commit v4 on v3

--- a/solution.py
+++ b/solution.py
@@ -18,15 +18,15 @@
 GROUP = 16
 TILES = SEQ // 128
 NN = (((1,), (0,)), ((), ()))
-N_COPIES = 106
+N_RECV, N_SEND = 50, 14
 
 
 def kernel(
     tok, ug, uv, gw, vw, gt, vt, hg,
-    own_o, cross_o, last_o, gwg_o, vwg_o, small_o,
+    base_o, last_o, gwg_o, vwg_o, small_o,
     TOK, UGI, UVI, HGI, GT, VT, SM, GW, KT, TS, UB, UBT, W, ACC, DA, DB, DA2, DB2,
-    RA0, RA1, RB0, RB1, SA0, SA1, SB0, SB1, PB, PX, RS, TX, TY, NC, NZ,
-    lsem, ssem, rsem,
+    RA0, RA1, RB0, RB1, SA0, SA1, SB0, SB1, PB, PX, RS, TX, TY, NC, NZ, BASE,
+    lsem, send_sem, recv_sem,
 ):
     y, x, z, c = (lax.axis_index(a) for a in ("y", "x", "z", "c"))
     p = 1 - c
@@ -34,18 +34,28 @@
     def ahead(i, k, n):
         return lax.rem(i + k, n)
 
-    ids = itertools.count()
-    started = []
-
-    def remote(src, dst, **dev):
-        i = next(ids)
-        copy = pltpu.make_async_remote_copy(
-            src_ref=src, dst_ref=dst, send_sem=ssem.at[i], recv_sem=rsem.at[i],
-            device_id=dev, device_id_type=MESH,
-        )
-        copy.start()
-        started.append(copy)
-        return copy
+    recv_ids, send_ids = itertools.count(), itertools.count()
+    sent = []
+
+    class Group:
+        def __init__(self, carrier):
+            self.carrier = carrier
+            self.sem = recv_sem.at[next(recv_ids)]
+
+        def wait(self):
+            pltpu.make_async_copy(self.carrier, self.carrier, self.sem).wait()
+
+    def family(carrier):
+        sem = send_sem.at[next(send_ids)]
+        sent.append((carrier, sem))
+
+        def remote(group, src, dst, **dev):
+            pltpu.make_async_remote_copy(
+                src_ref=src, dst_ref=dst, send_sem=sem, recv_sem=group.sem,
+                device_id=dev, device_id_type=MESH,
+            ).start()
+
+        return remote
 
     def load(src, dst, i):
         copy = pltpu.make_async_copy(src, dst, lsem.at[i])
@@ -75,23 +85,26 @@
 
     order_up = [(0, 0), (0, 1), (1, 0), (1, 1), (2, 0), (2, 1), (3, 0)]
     order_dn = [(s, 1 - h) for s, h in order_up]
-    up, down, cross = {}, {}, {}
+    around, cross = {}, {}
+    send_tok, send_cross = family(RS), family(TOK.at[pl.ds(0, 4)])
 
     def tok_send(j):
+        around[j] = Group(TOK.at[0, pl.ds(0, 128)])
         s, h = order_up[j]
         blk = tok_at(ahead(z, 8 - s, 8), c, h)
-        up[j] = remote(blk, blk, z=ahead(z, 1, 8))
+        send_tok(around[j], blk, blk, z=ahead(z, 1, 8))
         s, h = order_dn[j]
         blk = tok_at(ahead(z, s, 8), c, h)
-        down[j] = remote(blk, blk, z=ahead(z, 7, 8))
+        send_tok(around[j], blk, blk, z=ahead(z, 7, 8))
 
     def tok_cross(k, h):
+        if k not in cross:
+            cross[k] = Group(TOK.at[0, pl.ds(0, 128)])
         blk = tok_at(ahead(z, k, 8), c, h)
-        cross[k, h] = remote(blk, blk, c=p)
+        send_cross(cross[k], blk, blk, c=p)
 
     def tok_event(j):
-        up[j].wait_recv()
-        down[j].wait_recv()
+        around[j].wait()
         if j + 2 < 7:
             tok_send(j + 2)
         s, h = order_up[j]
@@ -104,24 +117,20 @@
     tok_cross(0, 0)
     tok_cross(0, 1)
 
-    def gather(slot, axis, i):
-        state = {}
+    def gather(remote, slot, axis, i, near_bytes, far_bytes):
+        near, far = Group(near_bytes), Group(far_bytes)
 
         def begin():
+            for s in (1, 3):
+                remote(near, slot(i, None), slot(i, None), **{axis: ahead(i, s, 4)})
+
+        def middle():
+            near.wait()
             for d, s in ((0, 1), (1, 3)):
-                state[d] = remote(slot(i, None), slot(i, None), **{axis: ahead(i, s, 4)})
-
-        def middle():
-            for d, s in ((0, 1), (1, 3)):
-                state[d].wait_recv()
-                far = ahead(i, 4 - s, 4)
-                state[2 + d] = remote(slot(far, d), slot(far, d), **{axis: ahead(i, s, 4)})
-
-        def end():
-            state[2].wait_recv()
-            state[3].wait_recv()
-
-        return begin, middle, end
+                blk = slot(ahead(i, 4 - s, 4), d)
+                remote(far, blk, blk, **{axis: ahead(i, s, 4)})
+
+        return begin, middle, far.wait
 
     quarter = WIDTH // 2
 
@@ -138,8 +147,17 @@
     def b2(i, d):
         return W.at[pl.ds(0, 4) if d is None else pl.ds(2 * d, 2), i, pl.ds(WIDTH, WIDTH)]
 
-    first = gather(a1, "x", x), gather(b1, "y", y)
-    second = gather(a2, "y", y), gather(b2, "x", x)
+    send_first, send_second = family(W.at[0, pl.ds(0, 3)]), family(W.at[pl.ds(0, 3)])
+    near1, far1 = W.at[0, 0], W.at[0, 0, pl.ds(0, WIDTH)]
+    near2, far2 = W.at[0], W.at[0, pl.ds(0, 2)]
+    first = (
+        gather(send_first, a1, "x", x, near1, far1),
+        gather(send_first, b1, "y", y, near1, far1),
+    )
+    second = (
+        gather(send_second, a2, "y", y, near2, far2),
+        gather(send_second, b2, "x", x, near2, far2),
+    )
     l_gw.wait()
     l_vw.wait()
     for g in first:
@@ -236,10 +254,10 @@
 
     def wait_cross(*ks):
         for k in ks:
-            cross[k, 0].wait_recv()
-            cross[k, 1].wait_recv()
+            cross[k].wait()
 
     partner = {}
+    send_part = family(PX)
 
     def input_part(k):
         zz = ahead(z, k, 8)
@@ -255,60 +273,66 @@
             return 0
 
         lax.fori_loop(0, 8, step, 0)
-        partner[k] = remote(PB.at[k, p], PX.at[k] if k else cross_o, c=p)
+        partner[k] = Group(PX.at[0])
+        send_part(partner[k], PB.at[k, p], PX.at[k], c=p)
 
     sum_up = [(0, 0), (1, 1), (1, 0), (2, 1), (2, 0), (3, 1), (3, 0)]
     flow = {}
-
-    def pair_sum(k, h, extra):
+    send_flow = family(RS)
+
+    def pair_sum(k, h, extra, dst=None):
         def step(i, _):
             rows = pl.ds(pl.multiple_of(h * 64 + i * 16, 16), 16)
             v = PB[k, c, rows, :].astype(F32) + PX[k, rows, :].astype(F32)
             if extra is not None:
                 v = v + RS[extra[0], extra[1], pl.ds(pl.multiple_of(i * 16, 16), 16), :].astype(F32)
-            PB[k, c, rows, :] = v.astype(BF16)
+            if dst is None:
+                PB[k, c, rows, :] = v.astype(BF16)
+            else:
+                dst[rows, :] = v.astype(BF16)
             return 0
 
         lax.fori_loop(0, 4, step, 0)
 
     def sum_event(j):
+        s = sum_up[j][0]
+        ks = (4 - s, 4 + s)
+        if j in (0, 1, 3, 5):
+            for k in sorted(set(ks)):
+                partner[k].wait()
+        if j >= 2:
+            flow[j - 2].wait()
+        flow[j] = Group(TOK.at[0, pl.ds(0, 128)])
         for d in range(2):
-            s, h = sum_up[j]
-            if d:
-                h = 1 - h
-            k = 4 - s if d == 0 else 4 + s
-            if j == 0 and d == 0 or j == 1 or j == 3 or j == 5:
-                partner[k].wait_recv()
-            if j >= 2:
-                flow[d, j - 2].wait_recv()
-            pair_sum(k, h, (d, j - 2) if j >= 2 else None)
-            flow[d, j] = remote(
-                PB.at[k, c, pl.ds(h * 64, 64)],
-                RS.at[d, j] if s < 3 else last_o.at[d, pl.ds(h * 64, 64)],
+            h = sum_up[j][1] if d == 0 else 1 - sum_up[j][1]
+            pair_sum(ks[d], h, (d, j - 2) if j >= 2 else None)
+            send_flow(
+                flow[j],
+                PB.at[ks[d], c, pl.ds(h * 64, 64)],
+                RS.at[d, j] if j < 6 else last_o.at[pl.ds(h * 64, 64)],
                 z=ahead(z, 1 if d == 0 else 7, 8),
             )
 
     def scatter(src, r0, r1, axis, i):
-        state = {}
         own = i
         near = {0: ahead(i, 1, 4), 1: ahead(i, 3, 4)}
         far = ahead(i, 2, 4)
+        remote = family(src.at[pl.ds(0, 3)])
+        early, late = Group(r0), Group(r1)
 
         def begin():
             for d in range(2):
                 to = {axis: near[d]}
-                state[d] = remote(src.at[far, d], r0.at[d], **to)
-                state[2 + d] = remote(src.at[near[d], 1 - d], r1.at[d, 1 - d], **to)
+                remote(early, src.at[far, d], r0.at[d], **to)
+                remote(late, src.at[near[d], 1 - d], r1.at[d, 1 - d], **to)
 
         def middle():
+            early.wait()
             for d in range(2):
-                state[d].wait_recv()
                 src[near[d], d] = (src[near[d], d].astype(F32) + r0[d].astype(F32)).astype(BF16)
-                state[4 + d] = remote(src.at[near[d], d], r1.at[d, d], **{axis: near[d]})
-
-        def end():
-            for i_ in range(2, 6):
-                state[i_].wait_recv()
+                remote(late, src.at[near[d], d], r1.at[d, d], **{axis: near[d]})
+
+        end = late.wait
 
         def total(*at):
             t = src[(own, *at)].astype(F32)
@@ -338,7 +362,9 @@
         for lo in range(0, WIDTH, 128):
             hi = min(lo + 128, WIDTH)
             TX[x, q, :, lo:hi] = TS[q, lo:hi, :].T[0:8]
-    tap_x = [remote(TX.at[x], TX.at[x], x=ahead(x, k, 4)) for k in (1, 2, 3)]
+    tap_x, send_x = Group(TX.at[pl.ds(0, 3)]), family(TX.at[pl.ds(0, 3)])
+    for k in (1, 2, 3):
+        send_x(tap_x, TX.at[x], TX.at[x], x=ahead(x, k, 4))
     lax.fori_loop(0, 8, lambda i, _: (turn(i), 0)[1], 0)
     tok_event(1)
     wait_cross(0)
@@ -348,10 +374,11 @@
     for g in second:
         g[1]()
     tok_event(2)
-    for copy in tap_x:
-        copy.wait_recv()
+    tap_x.wait()
     TY[y] = tap_sum(TX)
-    tap_y = [remote(TY.at[y], TY.at[y], y=ahead(y, k, 4)) for k in (1, 2, 3)]
+    tap_y, send_y = Group(TY.at[pl.ds(0, 3)]), family(TY.at[pl.ds(0, 3)])
+    for k in (1, 2, 3):
+        send_y(tap_y, TY.at[y], TY.at[y], y=ahead(y, k, 4))
     tok_event(3)
     for g in second:
         g[2]()
@@ -380,14 +407,16 @@
     sc_b1[1]()
     sum_event(3)
     input_part(0)
-    own = load(PB.at[0, c], own_o, 0)
-    for copy in tap_y:
-        copy.wait_recv()
+    tap_y.wait()
     taps = tap_sum(TY)
+    diagonal = lax.broadcasted_iota(jnp.int32, (8, 128), 0) == lax.broadcasted_iota(
+        jnp.int32, (8, 128), 1
+    )
+    NC[c] = jnp.zeros((4, 128), F32)
     for q in range(2):
         SM[8 * q : 8 * q + 8, :] = taps[q]
         square = jnp.sum(taps[q] * taps[q], axis=1, keepdims=True)
-        NC[c, 1 + q] = jnp.broadcast_to(square, (8, 128))
+        NC[c, 2 + q : 3 + q] = jnp.sum(jnp.where(diagonal, square, 0.0), axis=0, keepdims=True)
     sum_event(4)
     sc_a1[2]()
     sc_b1[2]()
@@ -401,42 +430,39 @@
     sum_event(5)
     sc_a2[2]()
     sc_b2[2]()
-    NC[c, 0] = jnp.zeros((8, 128), F32)
     for q, scat in enumerate((sc_a2, sc_b2)):
         grad = scat[3]().reshape(WIDTH, 128)
-        NC[c, 0, q : q + 1] = jnp.sum(grad * grad, axis=0, keepdims=True)
+        NC[c, q : q + 1] = jnp.sum(grad * grad, axis=0, keepdims=True)
         GW[q] = grad
-    pair = remote(NC.at[c], NC.at[c], c=p)
+    pair, send_pair = Group(NC.at[0]), family(NC.at[0])
+    send_pair(pair, NC.at[c], NC.at[c], c=p)
     results = [load(GW.at[0], gwg_o, 1), load(GW.at[1], vwg_o, 2)]
-    pair.wait_recv()
+    pair.wait()
     NZ[z] = NC[0] + NC[1]
-    along = [remote(NZ.at[z], NZ.at[z], z=ahead(z, k, 8)) for k in range(1, 8)]
+    along, send_along = Group(NZ.at[pl.ds(0, 7)]), family(NZ.at[pl.ds(0, 7)])
+    for k in range(1, 8):
+        send_along(along, NZ.at[z], NZ.at[z], z=ahead(z, k, 8))
     sum_event(6)
-    for copy in along:
-        copy.wait_recv()
+    partner[0].wait()
+    flow[5].wait()
+    pair_sum(0, 0, (1, 5), BASE)
+    pair_sum(0, 1, (0, 5), BASE)
+    base = load(BASE, base_o, 0)
+    along.wait()
     total = NZ[0]
     for k in range(1, 8):
         total = total + NZ[k]
-    diagonal = lax.broadcasted_iota(jnp.int32, (8, 128), 0) == lax.broadcasted_iota(
-        jnp.int32, (8, 128), 1
-    )
-    SM[16:24, 0:128] = total[0]
-    for q in range(2):
-        row = jnp.sum(jnp.where(diagonal, total[1 + q], 0.0), axis=0, keepdims=True)
-        SM[18 + q : 19 + q, 0:128] = row
+    SM[16:20, 0:128] = total
     small = load(SM, small_o, 3)
-    for copy in (own, *results, small):
+    for copy in (base, *results, small):
         copy.wait()
-    partner[0].wait_recv()
-    for d in range(2):
-        flow[d, 5].wait_recv()
-        flow[d, 6].wait_recv()
-    for copy in started:
-        copy.wait_send()
-    assert len(started) == N_COPIES, len(started)
-
-
-def finish(own, cross, last, gwg, vwg, small, ig_o, gwg_o, vwg_o, gtg_o, vtg_o, gn_o, vn_o, tn_o):
+    flow[6].wait()
+    for carrier, sem in sent:
+        pltpu.make_async_copy(carrier, carrier, sem).wait()
+    assert (next(recv_ids), next(send_ids)) == (N_RECV, N_SEND)
+
+
+def finish(base, last, gwg, vwg, small, ig_o, gwg_o, vwg_o, gtg_o, vtg_o, gn_o, vn_o, tn_o):
     gwg_o[...] = gwg[...]
     vwg_o[...] = vwg[...]
     gtg_o[...] = small[0:3, :]
@@ -444,8 +470,7 @@
     gn_o[...] = small[16:17, 0:128]
     vn_o[...] = small[17:18, 0:128]
     tn_o[...] = small[18:20, 0:3]
-    value = own[...].astype(F32) + cross[...].astype(F32)
-    ig_o[...] = (value + last[0].astype(F32) + last[1].astype(F32)).astype(BF16)
+    ig_o[...] = (base[...].astype(F32) + last[...].astype(F32)).astype(BF16)
 
 
 def local(tokens, up_gate, up_val, gate_weight, val_weight, gate_taps, val_taps, hidden_grad):
@@ -484,24 +509,24 @@
         pltpu.VMEM((2, 7, 64, D), BF16),
         pltpu.VMEM((4, 2, 8, WIDTH), F32),
         pltpu.VMEM((4, 2, 8, WIDTH), F32),
-        pltpu.VMEM((2, 3, 8, 128), F32),
-        pltpu.VMEM((8, 3, 8, 128), F32),
+        pltpu.VMEM((2, 4, 128), F32),
+        pltpu.VMEM((8, 4, 128), F32),
+        pltpu.VMEM((ROWS, D), BF16),
         pltpu.SemaphoreType.DMA((8,)),
-        pltpu.SemaphoreType.DMA((N_COPIES,)),
-        pltpu.SemaphoreType.DMA((N_COPIES,)),
+        pltpu.SemaphoreType.DMA((N_SEND,)),
+        pltpu.SemaphoreType.DMA((N_RECV,)),
     ]
     out = pl.pallas_call(
         kernel,
         out_shape=[
             jax.ShapeDtypeStruct((ROWS, D), BF16),
             jax.ShapeDtypeStruct((ROWS, D), BF16),
-            jax.ShapeDtypeStruct((2, ROWS, D), BF16),
             jax.ShapeDtypeStruct((WIDTH, ROWS), F32),
             jax.ShapeDtypeStruct((WIDTH, ROWS), F32),
             jax.ShapeDtypeStruct((24, WIDTH), F32),
         ],
         in_specs=[hbm] * 8,
-        out_specs=[hbm] * 6,
+        out_specs=[hbm] * 5,
         scratch_shapes=scratch,
         compiler_params=pltpu.CompilerParams(
             collective_id=0, has_side_effects=True, vmem_limit_bytes=67_000_000
@@ -520,7 +545,7 @@
             jax.ShapeDtypeStruct((1, ROWS), F32),
             jax.ShapeDtypeStruct((2, 3), F32),
         ],
-        in_specs=[vmem] * 6,
+        in_specs=[vmem] * 5,
         out_specs=[vmem] * 8,
         name="finish",
     )(*out)

time: 96.4 us -> 92.7 us (0.962)
  Pallas kernels: 95.6 us -> 91.9 us
    pallas_call x1, Pallas kernels: 92.9 us -> 89.7 us  [local(): pl.pallas_call(kernel, out_shape=[jax.ShapeDtypeStruct((ROWS, D), BF16),...]
where the time goes in v4:
time: 92.7 us; the launch traced here: 92.5 us
  Pallas kernels  91.9 us (99%)
    pallas_call x1, Pallas kernels, local(): pl.pallas_call(kernel, out_shape=[jax.ShapeDtypeStruct((ROWS, D), BF16),...  89.7 us
    pallas_call x1, Pallas kernels, local(): pl.pallas_call(finish, out_shape=[jax.ShapeDtypeStruct((ROWS, D), BF16),...  2.25 us

profile of v4, /device:TPU:1, one launch (start us, length us, event | category | flops | bytes accessed | tf_op | source)
XLA Modules:
  0.0 92.5 jit_solution(18396689194765035406)
XLA Ops:
  0.6 89.7 %backward.1 = (bf16[128,2048]{1,0:T(8,128)(2,1)}, bf16[128,2048]{1,0:T(8,128)(2,1)}, f32[352,128]{1,0:T(8,128)}, f32[352,128]{1,0:T(8,128)}, f32[24,352]{1,0:T(8,128)}) custom-call(bf16[128,2048]{1,0:T(8,128)(2,1)} %tok.1, bf16[352,2048]{1,0:T(8,128)(2,1)} %bitcast.9, bf16[352,2048]{1,0:T(8,128)(2,1)} %bitcast.10, bf16[352,128]{1,0:T(8,128)(2,1)} %bitcast.12, ...), custom_call_target="tpu_custom_call" | custom-call | tf_op jit(solution)/shard_map/backward/pallas_call | solution.py:519
  90.3 2.2 %finish.1 = (bf16[128,2048]{1,0:T(8,128)(2,1)}, f32[352,128]{1,0:T(8,128)}, f32[352,128]{1,0:T(8,128)}, f32[3,352]{1,0:T(4,128)}, f32[3,352]{1,0:T(4,128)}, /*in...) custom-call(bf16[128,2048]{1,0:T(8,128)(2,1)} %get-tuple-element.21.base, ...), custom_call_target="tpu_custom_call" | custom-call | tf_op jit(solution)/shard_map/finish/pallas_call | solution.py:536

commit v5 on v4

--- a/solution.py
+++ b/solution.py
@@ -18,13 +18,13 @@
 GROUP = 16
 TILES = SEQ // 128
 NN = (((1,), (0,)), ((), ()))
-N_RECV, N_SEND = 50, 14
+N_RECV, N_SEND = 44, 12
 
 
 def kernel(
     tok, ug, uv, gw, vw, gt, vt, hg,
-    base_o, last_o, gwg_o, vwg_o, small_o,
-    TOK, UGI, UVI, HGI, GT, VT, SM, GW, KT, TS, UB, UBT, W, ACC, DA, DB, DA2, DB2,
+    ig_o, gwg_o, vwg_o, gtg_o, vtg_o, gn_o, vn_o, tn_o,
+    TOK, UGI, UVI, HGI, GT, VT, KT, TS, UB, UBT, W, ACC, DA, DB, DA2, DB2,
     RA0, RA1, RB0, RB1, SA0, SA1, SB0, SB1, PB, PX, RS, TX, TY, NC, NZ, BASE,
     lsem, send_sem, recv_sem,
 ):
@@ -71,9 +71,9 @@
 
     barrier = pltpu.get_barrier_semaphore()
     peers = [{"c": p}]
-    peers += [{"x": ahead(x, k, 4)} for k in (1, 2, 3)]
-    peers += [{"y": ahead(y, k, 4)} for k in (1, 2, 3)]
-    peers += [{"z": ahead(z, k, 8)} for k in range(1, 8)]
+    peers += [{"x": ahead(x, k, 4)} for k in (1, 3)]
+    peers += [{"y": ahead(y, k, 4)} for k in (1, 3)]
+    peers += [{"z": ahead(z, k, 8)} for k in (1, 7)]
     for peer in peers:
         pl.semaphore_signal(barrier, inc=1, device_id=peer, device_id_type=MESH)
 
@@ -86,7 +86,7 @@
     order_up = [(0, 0), (0, 1), (1, 0), (1, 1), (2, 0), (2, 1), (3, 0)]
     order_dn = [(s, 1 - h) for s, h in order_up]
     around, cross = {}, {}
-    send_tok, send_cross = family(RS), family(TOK.at[pl.ds(0, 4)])
+    send_tok, send_cross = family(PB.at[pl.ds(0, 7)]), family(TOK)
 
     def tok_send(j):
         around[j] = Group(TOK.at[0, pl.ds(0, 128)])
@@ -99,7 +99,10 @@
 
     def tok_cross(k, h):
         if k not in cross:
-            cross[k] = Group(TOK.at[0, pl.ds(0, 128)])
+            alone = k in (0, 4)
+            cross[k] = Group(TOK.at[0, pl.ds(0, 128)] if alone else TOK.at[0])
+            if not alone:
+                cross[8 - k] = cross[k]
         blk = tok_at(ahead(z, k, 8), c, h)
         send_cross(cross[k], blk, blk, c=p)
 
@@ -253,11 +256,11 @@
         lax.fori_loop(0, 8, step, 0)
 
     def wait_cross(*ks):
-        for k in ks:
-            cross[k].wait()
+        for group in {id(cross[k]): cross[k] for k in ks}.values():
+            group.wait()
 
     partner = {}
-    send_part = family(PX)
+    send_part = send_cross
 
     def input_part(k):
         zz = ahead(z, k, 8)
@@ -273,12 +276,16 @@
             return 0
 
         lax.fori_loop(0, 8, step, 0)
-        partner[k] = Group(PX.at[0])
+        if k not in partner:
+            alone = k in (0, 4)
+            partner[k] = Group(PX.at[0] if alone else PX.at[pl.ds(0, 2)])
+            if not alone:
+                partner[8 - k] = partner[k]
         send_part(partner[k], PB.at[k, p], PX.at[k], c=p)
 
     sum_up = [(0, 0), (1, 1), (1, 0), (2, 1), (2, 0), (3, 1), (3, 0)]
     flow = {}
-    send_flow = family(RS)
+    send_flow = send_tok
 
     def pair_sum(k, h, extra, dst=None):
         def step(i, _):
@@ -298,8 +305,7 @@
         s = sum_up[j][0]
         ks = (4 - s, 4 + s)
         if j in (0, 1, 3, 5):
-            for k in sorted(set(ks)):
-                partner[k].wait()
+            partner[ks[0]].wait()
         if j >= 2:
             flow[j - 2].wait()
         flow[j] = Group(TOK.at[0, pl.ds(0, 128)])
@@ -309,7 +315,7 @@
             send_flow(
                 flow[j],
                 PB.at[ks[d], c, pl.ds(h * 64, 64)],
-                RS.at[d, j] if j < 6 else last_o.at[pl.ds(h * 64, 64)],
+                RS.at[d, j],
                 z=ahead(z, 1 if d == 0 else 7, 8),
             )
 
@@ -414,7 +420,7 @@
     )
     NC[c] = jnp.zeros((4, 128), F32)
     for q in range(2):
-        SM[8 * q : 8 * q + 8, :] = taps[q]
+        (gtg_o, vtg_o)[q][...] = taps[q, 0:3]
         square = jnp.sum(taps[q] * taps[q], axis=1, keepdims=True)
         NC[c, 2 + q : 3 + q] = jnp.sum(jnp.where(diagonal, square, 0.0), axis=0, keepdims=True)
     sum_event(4)
@@ -433,10 +439,9 @@
     for q, scat in enumerate((sc_a2, sc_b2)):
         grad = scat[3]().reshape(WIDTH, 128)
         NC[c, q : q + 1] = jnp.sum(grad * grad, axis=0, keepdims=True)
-        GW[q] = grad
+        (gwg_o, vwg_o)[q][...] = grad
     pair, send_pair = Group(NC.at[0]), family(NC.at[0])
     send_pair(pair, NC.at[c], NC.at[c], c=p)
-    results = [load(GW.at[0], gwg_o, 1), load(GW.at[1], vwg_o, 2)]
     pair.wait()
     NZ[z] = NC[0] + NC[1]
     along, send_along = Group(NZ.at[pl.ds(0, 7)]), family(NZ.at[pl.ds(0, 7)])
@@ -447,35 +452,39 @@
     flow[5].wait()
     pair_sum(0, 0, (1, 5), BASE)
     pair_sum(0, 1, (0, 5), BASE)
-    base = load(BASE, base_o, 0)
     along.wait()
     total = NZ[0]
     for k in range(1, 8):
         total = total + NZ[k]
-    SM[16:20, 0:128] = total
-    small = load(SM, small_o, 3)
-    for copy in (base, *results, small):
-        copy.wait()
+    gn_o[...] = total[0:1]
+    vn_o[...] = total[1:2]
+    tn_o[...] = total[2:4, 0:3]
     flow[6].wait()
+
+    def last(i, _):
+        for d in range(2):
+            rows = pl.ds(pl.multiple_of(d * 64 + i * 16, 16), 16)
+            here = pl.ds(pl.multiple_of(i * 16, 16), 16)
+            ig_o[rows, :] = (BASE[rows, :].astype(F32) + RS[d, 6, here, :].astype(F32)).astype(BF16)
+        return 0
+
+    lax.fori_loop(0, 4, last, 0)
     for carrier, sem in sent:
         pltpu.make_async_copy(carrier, carrier, sem).wait()
     assert (next(recv_ids), next(send_ids)) == (N_RECV, N_SEND)
 
 
-def finish(base, last, gwg, vwg, small, ig_o, gwg_o, vwg_o, gtg_o, vtg_o, gn_o, vn_o, tn_o):
-    gwg_o[...] = gwg[...]
-    vwg_o[...] = vwg[...]
-    gtg_o[...] = small[0:3, :]
-    vtg_o[...] = small[8:11, :]
-    gn_o[...] = small[16:17, 0:128]
-    vn_o[...] = small[17:18, 0:128]
-    tn_o[...] = small[18:20, 0:3]
-    ig_o[...] = (base[...].astype(F32) + last[...].astype(F32)).astype(BF16)
+def finish(*refs):
+    srcs, dsts, sem = refs[:8], refs[8:16], refs[16]
+    copies = [pltpu.make_async_copy(a, b, sem.at[i]) for i, (a, b) in enumerate(zip(srcs, dsts))]
+    for c in copies:
+        c.start()
+    for c in copies:
+        c.wait()
 
 
 def local(tokens, up_gate, up_val, gate_weight, val_weight, gate_taps, val_taps, hidden_grad):
     hbm = pl.BlockSpec(memory_space=pl.ANY)
-    vmem = pl.BlockSpec(memory_space=pltpu.VMEM)
     half = WIDTH // 2
     scratch = [
         pltpu.VMEM((8, 256, D), BF16),
@@ -484,8 +493,6 @@
         pltpu.VMEM((WIDTH, 2 * SEQ), BF16),
         pltpu.VMEM((3, WIDTH), BF16),
         pltpu.VMEM((3, WIDTH), BF16),
-        pltpu.VMEM((24, WIDTH), F32),
-        pltpu.VMEM((2, WIDTH, ROWS), F32),
         pltpu.VMEM((2, WIDTH, 128), F32),
         pltpu.VMEM((2, WIDTH, 128), F32),
         pltpu.VMEM((2 * SEQ, BOTH), BF16),
@@ -516,37 +523,39 @@
         pltpu.SemaphoreType.DMA((N_SEND,)),
         pltpu.SemaphoreType.DMA((N_RECV,)),
     ]
+    shapes = [
+        jax.ShapeDtypeStruct((ROWS, D), BF16),
+        jax.ShapeDtypeStruct((WIDTH, ROWS), F32),
+        jax.ShapeDtypeStruct((WIDTH, ROWS), F32),
+        jax.ShapeDtypeStruct((3, WIDTH), F32),
+        jax.ShapeDtypeStruct((3, WIDTH), F32),
+        jax.ShapeDtypeStruct((1, ROWS), F32),
+        jax.ShapeDtypeStruct((1, ROWS), F32),
+        jax.ShapeDtypeStruct((2, 3), F32),
+    ]
+    vmem = pl.BlockSpec(memory_space=pltpu.VMEM)
+    args = (
+        tokens, up_gate.T, up_val.T, gate_weight.T, val_weight.T, gate_taps, val_taps, hidden_grad.T,
+    )
+    kept = [pltpu.with_memory_space_constraint(a, pltpu.HBM) for a in args]
     out = pl.pallas_call(
         kernel,
-        out_shape=[
-            jax.ShapeDtypeStruct((ROWS, D), BF16),
-            jax.ShapeDtypeStruct((ROWS, D), BF16),
-            jax.ShapeDtypeStruct((WIDTH, ROWS), F32),
-            jax.ShapeDtypeStruct((WIDTH, ROWS), F32),
-            jax.ShapeDtypeStruct((24, WIDTH), F32),
-        ],
+        out_shape=shapes,
         in_specs=[hbm] * 8,
-        out_specs=[hbm] * 5,
+        out_specs=[vmem] * 8,
         scratch_shapes=scratch,
         compiler_params=pltpu.CompilerParams(
-            collective_id=0, has_side_effects=True, vmem_limit_bytes=67_000_000
+            collective_id=0, has_side_effects=True, vmem_limit_bytes=54000000
         ),
         name="backward",
-    )(tokens, up_gate.T, up_val.T, gate_weight.T, val_weight.T, gate_taps, val_taps, hidden_grad.T)
+    )(*kept)
     out = pl.pallas_call(
         finish,
-        out_shape=[
-            jax.ShapeDtypeStruct((ROWS, D), BF16),
-            jax.ShapeDtypeStruct((WIDTH, ROWS), F32),
-            jax.ShapeDtypeStruct((WIDTH, ROWS), F32),
-            jax.ShapeDtypeStruct((3, WIDTH), F32),
-            jax.ShapeDtypeStruct((3, WIDTH), F32),
-            jax.ShapeDtypeStruct((1, ROWS), F32),
-            jax.ShapeDtypeStruct((1, ROWS), F32),
-            jax.ShapeDtypeStruct((2, 3), F32),
-        ],
-        in_specs=[vmem] * 5,
-        out_specs=[vmem] * 8,
+        out_shape=shapes,
+        in_specs=[vmem] * 8,
+        out_specs=[hbm] * 8,
+        scratch_shapes=[pltpu.SemaphoreType.DMA((8,))],
+        compiler_params=pltpu.CompilerParams(vmem_limit_bytes=4_000_000),
         name="finish",
     )(*out)
     return (out[0], out[1].T, out[2].T, out[3], out[4], out[5].reshape(ROWS), out[6].reshape(ROWS), out[7])

time: 92.7 us -> 90.9 us (0.981)
  Pallas kernels: 91.9 us -> 90.2 us
    pallas_call x2, Pallas kernels: 91.9 us -> 90.2 us  [the longest x1 89.2 us: local(): pl.pallas_call(kernel, out_shape=shapes, in_specs=[hbm] * 8, out_specs=[v...]
where the time goes in v5:
time: 90.9 us; the launch traced here: 90.8 us
  Pallas kernels  90.2 us (99%)
    pallas_call x1, Pallas kernels, local(): pl.pallas_call(kernel, out_shape=shapes, in_specs=[hbm] * 8, out_specs=[v...  89.2 us

profile of v5, /device:TPU:1, one launch (start us, length us, event | category | flops | bytes accessed | tf_op | source)
XLA Modules:
  0.0 90.8 jit_solution(16814771881373821199)
XLA Ops:
  0.6 89.2 %backward.1 = (bf16[128,2048]{1,0:T(8,128)(2,1)S(1)}, f32[352,128]{1,0:T(8,128)S(1)}, f32[352,128]{1,0:T(8,128)S(1)}, f32[3,352]{1,0:T(4,128)S(1)}, f32[3,352]{1...) custom-call(bf16[128,2048]{1,0:T(8,128)(2,1)} %tok.1, bf16[352,2048]{1,0:T(8,128)(2,1)} %bitcast.9, ...), custom_call_target="tpu_custom_call" | custom-call | tf_op jit(solution)/shard_map/backward/pallas_call | solution.py:541
  89.8 1.0 %finish.1 = (bf16[128,2048]{1,0:T(8,128)(2,1)}, f32[352,128]{1,0:T(8,128)}, f32[352,128]{1,0:T(8,128)}, f32[3,352]{1,0:T(4,128)}, f32[3,352]{1,0:T(4,128)}, /*in...) custom-call(bf16[128,2048]{1,0:T(8,128)(2,1)S(1)} %get-tuple-element.24.refs_0_, ...), custom_call_target="tpu_custom_call" | custom-call | tf_op jit(solution)/shard_map/finish/pallas_call | solution.py:552

commit v6 on v5

--- a/solution.py
+++ b/solution.py
@@ -18,7 +18,7 @@
 GROUP = 16
 TILES = SEQ // 128
 NN = (((1,), (0,)), ((), ()))
-N_RECV, N_SEND = 44, 12
+N_RECV, N_SEND = 44, 14
 
 
 def kernel(
@@ -49,6 +49,9 @@
         sem = send_sem.at[next(send_ids)]
         sent.append((carrier, sem))
 
+        return sender(sem)
+
+    def sender(sem):
         def remote(group, src, dst, **dev):
             pltpu.make_async_remote_copy(
                 src_ref=src, dst_ref=dst, send_sem=sem, recv_sem=group.sem,
@@ -86,9 +89,42 @@
     order_up = [(0, 0), (0, 1), (1, 0), (1, 1), (2, 0), (2, 1), (3, 0)]
     order_dn = [(s, 1 - h) for s, h in order_up]
     around, cross = {}, {}
-    send_tok, send_cross = family(PB.at[pl.ds(0, 7)]), family(TOK)
+    send_tok, send_cross = family(RS.at[pl.ds(0, 2), pl.ds(0, 6)]), family(TOK)
+
+    edge_sem = send_sem.at[next(send_ids)]
+    send_edge = sender(edge_sem)
+
+    def tok_last():
+        around[6] = Group(TOK.at[0, pl.ds(0, 128)])
+        blk = tok_at(ahead(z, 3, 8), c, 1)
+        send_edge(around[6], blk, blk, z=ahead(z, 7, 8))
+        zz, top = ahead(z, 5, 8), pl.multiple_of(c * ROWS, ROWS)
+        blk = TOK.at[zz, pl.ds(top, 48)]
+        send_edge(around[6], blk, blk, z=ahead(z, 1, 8))
+
+        @pl.when(z != 7)
+        def _():
+            rest = TOK.at[zz, pl.ds(pl.multiple_of(top + 48, 16), 16)]
+            send_edge(around[6], rest, rest, z=ahead(z, 1, 8))
+
+    def tok_extra():
+        @pl.when(z == 1)
+        def _():
+            rest = TOK.at[ahead(z, 3, 8), pl.ds(pl.multiple_of(c * ROWS + 48, 16), 16)]
+            send_edge(around[6], rest, rest, z=ahead(z, 7, 8))
+
+    def tok_last_wait():
+        for case, rows in ((z == 7, 112), (z == 1, 144), ((z != 7) & (z != 1), 128)):
+
+            @pl.when(case)
+            def _(rows=rows):
+                blk = TOK.at[0, pl.ds(0, rows)]
+                pltpu.make_async_copy(blk, blk, edge_sem).wait()
 
     def tok_send(j):
+        if j == 6:
+            tok_last()
+            return
         around[j] = Group(TOK.at[0, pl.ds(0, 128)])
         s, h = order_up[j]
         blk = tok_at(ahead(z, 8 - s, 8), c, h)
@@ -110,6 +146,8 @@
         around[j].wait()
         if j + 2 < 7:
             tok_send(j + 2)
+        if j == 5:
+            tok_extra()
         s, h = order_up[j]
         tok_cross(7 - s, h)
         s, h = order_dn[j]
@@ -285,7 +323,7 @@
 
     sum_up = [(0, 0), (1, 1), (1, 0), (2, 1), (2, 0), (3, 1), (3, 0)]
     flow = {}
-    send_flow = send_tok
+    send_flow = family(RS)
 
     def pair_sum(k, h, extra, dst=None):
         def step(i, _):
@@ -469,6 +507,7 @@
         return 0
 
     lax.fori_loop(0, 4, last, 0)
+    tok_last_wait()
     for carrier, sem in sent:
         pltpu.make_async_copy(carrier, carrier, sem).wait()
     assert (next(recv_ids), next(send_ids)) == (N_RECV, N_SEND)

time: 90.9 us -> 95.4 us (1.050)
  Pallas kernels: 90.2 us -> 94.7 us
    pallas_call x1, Pallas kernels: 89.2 us -> 93.7 us  [local(): pl.pallas_call(kernel, out_shape=shapes, in_specs=[hbm] * 8, out_specs=[v...]
where the time goes in v6:
time: 95.4 us
  Pallas kernels  94.7 us (99%)
    pallas_call x1, Pallas kernels, local(): pl.pallas_call(kernel, out_shape=shapes, in_specs=[hbm] * 8, out_specs=[v...  93.7 us

profile of v6, /device:TPU:1, one launch (start us, length us, event | category | flops | bytes accessed | tf_op | source)
XLA Modules:
  0.0 95.4 jit_solution(1302186071917096934)
XLA Ops:
  0.6 93.7 %backward.1 = (bf16[128,2048]{1,0:T(8,128)(2,1)S(1)}, f32[352,128]{1,0:T(8,128)S(1)}, f32[352,128]{1,0:T(8,128)S(1)}, f32[3,352]{1,0:T(4,128)S(1)}, f32[3,352]{1...) custom-call(bf16[128,2048]{1,0:T(8,128)(2,1)} %tok.1, bf16[352,2048]{1,0:T(8,128)(2,1)} %bitcast.9, ...), custom_call_target="tpu_custom_call" | custom-call | tf_op jit(solution)/shard_map/backward/pallas_call | solution.py:580
  94.4 1.0 %finish.1 = (bf16[128,2048]{1,0:T(8,128)(2,1)}, f32[352,128]{1,0:T(8,128)}, f32[352,128]{1,0:T(8,128)}, f32[3,352]{1,0:T(4,128)}, f32[3,352]{1,0:T(4,128)}, /*in...) custom-call(bf16[128,2048]{1,0:T(8,128)(2,1)S(1)} %get-tuple-element.24.refs_0_, ...), custom_call_target="tpu_custom_call" | custom-call | tf_op jit(solution)/shard_map/finish/pallas_call | solution.py:591
